TPU v7x, 32 devices: a whole 2x2x4 slice. The times are simulated.
32 devices in a mesh: grp: 2 (over y), sp: 4 (over z), tp: 4 (over x, core).
Axes of the slice: x: 2, y: 2, z: 4, core: 2. Of those that a mesh axis runs over, the one named last changes fastest.
Arguments:
- queries: bfloat16 [4096, 2048], P(('grp', 'sp'), 'tp'), parts along dimension 0, may hold values from -64 to 64
- key_heads: bfloat16 [4096, 4, 64], P(('grp', 'sp'), 'tp'), parts along dimension 0, may hold values from -64 to 64
- value_heads: bfloat16 [4096, 4, 64], P(('grp', 'sp'), 'tp'), parts along dimension 0, may hold values from -6 to 6
- sink_logit: float32 [32], P('tp'), may hold values from 3 to 6
- out_weight: bfloat16 [2048, 2048], P('tp'), may hold values from -0.75 to 0.75
- residual: bfloat16 [4096, 2048], P(('grp', 'sp', 'tp')), parts along dimension 0, may hold values from -6 to 6
- norm_gain: float32 [2048], replicated, may hold values from 0.1 to 1.9
- expert_ids: int32 [4096, 2], P(('grp', 'sp', 'tp')), parts along dimension 0, may hold values from 0 to 15, all different within a row; in each aligned block of 128 rows (0 to 127, 128 to 255, ...) at most 32 rows name the same one
- route_weights: float32 [4096, 2], P(('grp', 'sp', 'tp')), parts along dimension 0, may hold values from 0.1 to 1
- gate_weight: bfloat16 [16, 2048, 512], P(('sp', 'tp')), may hold values from -0.125 to 0.125
- up_weight: bfloat16 [16, 2048, 512], P(('sp', 'tp')), may hold values from -0.125 to 0.125
- down_weight: bfloat16 [16, 512, 2048], P(('sp', 'tp')), may hold values from -0.5 to 0.5
Outputs:
- mixed: bfloat16 [4096, 2048], P(('grp', 'sp', 'tp')), parts along dimension 0
There are 2 independent parts, one for each index of `grp`. A program takes and returns all parts, laid end to end along the dimension named above; an argument that names none is the same for every part. Nothing has to cross between parts.
Inputs may be any that keep to these rules, and one draw needn't show every extreme that they name: `expert_ids`: each row names 2 different experts. In the rows of one device (aligned blocks of 128 rows) no expert is named more than 32 times, and in some blocks one expert is named exactly 32 times.
All inputs are finite; a program needn't handle non-finite values.
Results may differ from a plain program's by a relative error of at most 0.014.
Values may be sent and summed in bfloat16 or wider, within the bound.
A program may use at most 64 MiB of HBM per device.

v0:
```python
import functools

import jax
import jax.numpy as jnp
from jax import lax
from jax.experimental import pallas as pl
from jax.experimental.pallas import tpu as pltpu
from jax.sharding import PartitionSpec as P

WINDOW = 128


EPS = 1e-06

F32 = jnp.float32
BF16 = jnp.bfloat16
MESH = pl.DeviceIdType.MESH
VMEM_BUDGET = 56 * 1024 * 1024


def from_behind(value, axis, steps):
    count = lax.axis_size(axis)
    initial, last = (max(0, -steps), min(count, count - steps))
    return lax.ppermute(value, axis, [(source, source + steps) for source in range(initial, last)])


def dot(a, b, dims=((1,), (0,))):
    return lax.dot_general(a, b, (dims, ((), ())), preferred_element_type=F32)


def attention(queries, key_heads, value_heads, sink_logit):
    rows_sp = queries.shape[0]
    kv_local = key_heads.shape[1]
    head_dim = key_heads.shape[2]
    heads_local = queries.shape[1] // head_dim
    group_size = heads_local // kv_local
    window = WINDOW
    count_of_blocks = rows_sp // window
    edge = jnp.stack([key_heads[rows_sp - window :], value_heads[rows_sp - window :]])
    tail_rows = from_behind(edge, "sp", 1)
    key_blocks = jnp.concatenate([tail_rows[0], key_heads], 0).reshape(
        count_of_blocks + 1, window, kv_local, head_dim
    )
    value_blocks = jnp.concatenate([tail_rows[1], value_heads], 0).reshape(
        count_of_blocks + 1, window, kv_local, head_dim
    )
    key_span = jnp.concatenate([key_blocks[:-1], key_blocks[1:]], 1)
    value_span = jnp.concatenate([value_blocks[:-1], value_blocks[1:]], 1)
    query_pos = jnp.arange(window, dtype=jnp.int32)[:, None]
    key_pos = jnp.arange(2 * window, dtype=jnp.int32)[None, :]
    distance = query_pos + window - key_pos
    band = (distance >= 0) & (distance < window)
    key_start = (
        lax.axis_index("sp") * rows_sp
        + jnp.arange(count_of_blocks, dtype=jnp.int32)[:, None] * window
        - window
        + key_pos
    )
    allowed = band[None, :, :] & (key_start >= 0)[:, None, :]
    query_blocks = queries.reshape(count_of_blocks, window, kv_local, group_size, head_dim)
    logit_scores = jnp.einsum(
        "bqhgd,bkhd->bhgqk", query_blocks, key_span, preferred_element_type=jnp.float32
    ) * head_dim ** (-0.5)
    logit_scores = jnp.where(allowed[:, None, None], logit_scores, -jnp.inf)
    sink_col = sink_logit.reshape(kv_local, group_size)[None, :, :, None, None]
    row_max = jnp.maximum(jnp.max(logit_scores, axis=-1, keepdims=True), sink_col)
    expd = jnp.exp(logit_scores - row_max)
    row_total = jnp.sum(expd, axis=-1, keepdims=True) + jnp.exp(sink_col - row_max)
    attention_probabilities = (expd / row_total).astype(jnp.bfloat16)
    attended = jnp.einsum(
        "bhgqk,bkhd->bqhgd", attention_probabilities, value_span, preferred_element_type=jnp.float32
    ).astype(jnp.bfloat16)
    return attended.reshape(rows_sp, heads_local * head_dim)


def tail_plain(
    attended, out_weight, residual, norm_gain, expert_ids, route_weights,
    gate_weight, up_weight, down_weight,
):
    rows_dev = residual.shape[0]
    width = residual.shape[1]
    projected = lax.psum_scatter(
        jnp.dot(attended, out_weight, preferred_element_type=jnp.float32),
        "tp",
        scatter_dimension=0,
        tiled=True,
    )
    stream = (residual.astype(jnp.float32) + projected).astype(jnp.bfloat16)
    wide = stream.astype(jnp.float32)
    normed = (
        wide * lax.rsqrt(jnp.mean(wide * wide, axis=-1, keepdims=True) + EPS) * norm_gain
    ).astype(jnp.bfloat16)
    sp_count = lax.axis_size("sp")
    tp_count = lax.axis_size("tp")
    experts_total = sp_count * tp_count
    top_k = expert_ids.shape[1]
    capacity = max(2, 2 * top_k * rows_dev // experts_total)
    flat_ids = expert_ids.reshape(-1)
    pairs = flat_ids.shape[0]
    onehot = (flat_ids[:, None] == jnp.arange(experts_total, dtype=jnp.int32)[None, :]).astype(
        jnp.int32
    )
    earlier = jnp.cumsum(onehot, axis=0) - onehot
    slot_rank = jnp.sum(earlier * onehot, axis=1)
    flat_slot = flat_ids * capacity + slot_rank
    owner_row = jnp.arange(pairs, dtype=jnp.int32) // top_k
    token_in_slot = jnp.zeros((experts_total * capacity,), jnp.int32).at[flat_slot].set(owner_row)
    filled = jnp.zeros((experts_total * capacity,), jnp.bool_).at[flat_slot].set(True)
    outbox = jnp.where(filled[:, None], normed[token_in_slot], jnp.zeros((), jnp.bfloat16))
    outbox = outbox.reshape(experts_total, capacity, width)
    arrived = lax.all_to_all(outbox, ("sp", "tp"), split_axis=0, concat_axis=0, tiled=True)
    rows = arrived.reshape(-1, width)
    gate = jnp.dot(rows, gate_weight[0], preferred_element_type=jnp.float32)
    upward = jnp.dot(rows, up_weight[0], preferred_element_type=jnp.float32)
    expert_hidden = (jax.nn.silu(gate) * upward).astype(jnp.bfloat16)
    expert_rows = jnp.dot(expert_hidden, down_weight[0], preferred_element_type=jnp.float32).astype(
        jnp.bfloat16
    )
    results = expert_rows.reshape(arrived.shape)
    returned = lax.all_to_all(results, ("sp", "tp"), split_axis=0, concat_axis=0, tiled=True)
    picked_rows = returned.reshape(experts_total * capacity, width)[flat_slot].reshape(
        rows_dev, top_k, width
    )
    shares = route_weights / jnp.sum(route_weights, axis=-1, keepdims=True)
    combined = jnp.sum(shares[:, :, None] * picked_rows.astype(jnp.float32), axis=1)
    return (wide + combined).astype(jnp.bfloat16)


def routing(ids, weights, experts, capacity):
    top_k, rows = ids.shape
    pad = jnp.zeros((-2 * top_k % 8, rows), F32)
    facts = jnp.concatenate([ids.astype(F32), weights, pad], 0).T
    ids, weights = facts[:, :top_k], facts[:, top_k : 2 * top_k]
    expert = lax.broadcasted_iota(jnp.int32, (rows, experts), 1).astype(F32)
    total = jnp.sum(weights, axis=1, keepdims=True)
    member = jnp.zeros((rows, experts), F32)
    share = jnp.zeros((rows, experts), F32)
    for k in range(top_k):
        hit = jnp.where(ids[:, k : k + 1] == expert, 1.0, 0.0)
        member = member + hit
        share = share + hit * (weights[:, k : k + 1] / total)
    before = (
        lax.broadcasted_iota(jnp.int32, (rows, rows), 0)
        > lax.broadcasted_iota(jnp.int32, (rows, rows), 1)
    ).astype(BF16)
    rank = dot(before, member.astype(BF16))
    rank = jnp.where(member > 0, rank, -1.0)
    slots = experts * capacity
    spread = (
        lax.broadcasted_iota(jnp.int32, (experts, slots), 1) // capacity
        == lax.broadcasted_iota(jnp.int32, (experts, slots), 0)
    ).astype(BF16)
    rank_slot = dot(rank.astype(BF16), spread)
    place = lax.broadcasted_iota(jnp.int32, (rows, slots), 1) % capacity
    taken = rank_slot == place.astype(F32)
    high = share.astype(BF16)
    low = (share - high.astype(F32)).astype(BF16)
    one = jnp.where(taken, 1.0, 0.0)
    return (
        one.astype(BF16),
        (one * dot(high, spread)).astype(BF16),
        (one * dot(low, spread)).astype(BF16),
    )


def attend(z, token_rows, queries, sink, seen, attended, at):
    window = WINDOW
    rows, lanes = queries.shape[0], seen.shape[1]
    heads = sink.shape[1]
    size = queries.shape[1] // heads
    groups = lanes // (2 * size)
    share = heads // groups
    pairs = share // 2
    tall = pairs * window
    query = lax.broadcasted_iota(jnp.int32, (tall, 2 * window), 0) % window
    key = lax.broadcasted_iota(jnp.int32, (tall, 2 * window), 1)
    distance = query + window - key
    band = (distance >= 0) & (distance < window)

    def block(b):
        allowed = band & ((z * rows + b * window - window) + key >= 0)
        span = seen[pl.ds(pl.multiple_of(b * window, window), 2 * window), :]
        here = pl.ds(pl.multiple_of(b * window, window), window)
        for g in range(groups):
            keys = span[:, 2 * g * size : (2 * g + 1) * size]
            values = span[:, (2 * g + 1) * size : (2 * g + 2) * size]
            none, ones = jnp.zeros_like(keys), jnp.ones_like(values)
            wide = jnp.concatenate(
                [
                    queries[here, (g * share + 2 * i) * size : (g * share + 2 * i + 2) * size]
                    for i in range(pairs)
                ],
                0,
            )
            sides = []
            for odd in range(2):
                two_keys = jnp.concatenate([none, keys] if odd else [keys, none], 1)
                two_values = jnp.concatenate([ones, values] if odd else [values, ones], 1)
                score = dot(wide, two_keys, ((1,), (1,))) * size**-0.5
                score = jnp.where(allowed, score, -1e30)
                drain = jnp.concatenate(
                    [
                        jnp.broadcast_to(
                            sink[0:1, g * share + 2 * i + odd : g * share + 2 * i + odd + 1],
                            (window, 1),
                        )
                        for i in range(pairs)
                    ],
                    0,
                )
                top = jnp.maximum(jnp.max(score, axis=1, keepdims=True), drain)
                grown = jnp.exp(score - top).astype(BF16)
                both = dot(grown, two_values)
                at = 0 if odd else size
                total = both[:, at : at + 1] + jnp.exp(drain - top)
                sides.append(both * (1.0 / total))
            lane = lax.broadcasted_iota(jnp.int32, (tall, 2 * size), 1)
            both = jnp.where(lane < size, sides[0], sides[1]).astype(BF16)
            for i in range(pairs):
                first = (g * share + 2 * i) * size
                attended[here, first : first + 2 * size] = both[i * window : (i + 1) * window]

    for b in range(token_rows // window):
        block(at * (token_rows // window) + b)


def tail_kernel(
    sizes,
    queries, kv, sink, out_w_hbm, residual, gain, ids, weights, gate_hbm, up_hbm, down_hbm,
    out,
    seen, attended, halo_send, halo_recv,
    out_w, gate_w, up_w, down_w,
    pair_out, pair_in, far_out, far_in,
    stream, normed, slots, share_hi, share_lo,
    outbox, arrived, results, returned,
    load_sem, pair_send, pair_recv, far_send, far_recv,
    go_send, go_recv, back_send, back_recv,
):
    sp_count, tp_count, pieces, capacity = sizes
    experts = sp_count * tp_count
    chips = tp_count // 2
    z, t = lax.axis_index("sp"), lax.axis_index("tp")
    me = z * tp_count + t
    x, core = t // 2, t % 2
    other = 1 - core
    rows, width = residual.shape
    piece = width // pieces

    def where(e):
        return {"sp": e // tp_count, "tp": e % tp_count}

    loads = [
        pltpu.make_async_copy(src, dst, load_sem.at[i])
        for i, (src, dst) in enumerate(
            ((out_w_hbm, out_w), (gate_hbm.at[0], gate_w), (up_hbm.at[0], up_w), (down_hbm.at[0], down_w))
        )
    ]
    for load in loads:
        load.start()

    barrier = pltpu.get_barrier_semaphore()

    def greet(k, carry):
        pl.semaphore_signal(
            barrier, inc=1, device_id=where((me + k) % experts), device_id_type=MESH
        )
        return carry

    lax.fori_loop(1, experts, greet, 0)
    pl.semaphore_wait(barrier, experts - 1)
    reach = kv.shape[0]
    halo_copy = pltpu.make_async_remote_copy(
        kv.at[pl.ds(reach - WINDOW, WINDOW)], seen.at[pl.ds(0, WINDOW)], halo_send, halo_recv,
        device_id={"sp": jnp.minimum(z + 1, sp_count - 1)}, device_id_type=MESH,
    )

    @pl.when(z < sp_count - 1)
    def _():
        halo_copy.start()

    seen[WINDOW:, :] = kv[...]
    slots[...], share_hi[...], share_lo[...] = routing(ids[...], weights[...], experts, capacity)

    @pl.when(z == 0)
    def _():
        seen[:WINDOW, :] = jnp.zeros((WINDOW, kv.shape[1]), BF16)

    @pl.when(z > 0)
    def _():
        halo_copy.wait_recv()

    loads[0].wait()

    def partial(chip, which, q):
        block = attended[pl.ds(pl.multiple_of((chip * 2 + which) * rows, rows), rows), :]
        return dot(block, out_w[:, q * piece : (q + 1) * piece])

    def pair_copy(k, q):
        return pltpu.make_async_remote_copy(
            pair_out.at[k, q], pair_in.at[k, q], pair_send.at[k, q], pair_recv.at[k, q],
            device_id={"tp": x * 2 + other}, device_id_type=MESH,
        )

    def far_copy(k, q):
        return pltpu.make_async_remote_copy(
            far_out.at[k, q], far_in.at[k, q], far_send.at[k, q], far_recv.at[k, q],
            device_id={"tp": ((x + k) % chips) * 2 + core}, device_id_type=MESH,
        )

    order = list(range(1, chips)) + [0]
    for k in order:
        chip = (x + k) % chips
        attend(z, rows, queries, sink, seen, attended, chip * 2 + other)
        for q in range(pieces):
            pair_out[k, q] = partial(chip, other, q).astype(BF16)
            pair_copy(k, q).start()
        attend(z, rows, queries, sink, seen, attended, chip * 2 + core)
        for q in range(pieces if k else 0):
            mine = partial(chip, core, q)
            pair_copy(k, q).wait_recv()
            far_out[k, q] = (mine + pair_in[k, q].astype(F32)).astype(BF16)
            far_copy(k, q).start()
    square = jnp.zeros((rows, 1), F32)
    for q in range(pieces):
        cols = slice(q * piece, (q + 1) * piece)
        total = partial(x, core, q)
        pair_copy(0, q).wait_recv()
        total = total + pair_in[0, q].astype(F32)
        for k in range(1, chips):
            far_copy(k, q).wait_recv()
            total = total + far_in[k, q].astype(F32)
        value = (residual[:, cols].astype(F32) + total).astype(BF16)
        stream[:, cols] = value
        value = value.astype(F32)
        square = square + jnp.sum(value * value, axis=1, keepdims=True)
    scale = lax.rsqrt(square / width + EPS)
    for q in range(pieces):
        cols = slice(q * piece, (q + 1) * piece)
        normed[:, cols] = (stream[:, cols].astype(F32) * scale * gain[:, cols]).astype(BF16)

    def go_copy(to, at):
        return pltpu.make_async_remote_copy(
            outbox.at[to], arrived.at[at], go_send.at[to], go_recv.at[at],
            device_id=where(to), device_id_type=MESH,
        )

    def back_copy(to, at):
        return pltpu.make_async_remote_copy(
            results.at[to], returned.at[at], back_send.at[to], back_recv.at[at],
            device_id=where(to), device_id_type=MESH,
        )

    picks = tp_count * capacity
    for d in range(sp_count):
        layer = range(d * tp_count, (d + 1) * tp_count)
        chosen = dot(slots[:, d * picks : (d + 1) * picks], normed[...], ((0,), (0,))).astype(BF16)
        for i, e in enumerate(layer):
            outbox[e] = chosen[i * capacity : (i + 1) * capacity]

            @pl.when(e != me)
            def _():
                go_copy(e, me).start()

    arrived[me] = outbox[me]
    for load in loads[1:]:
        load.wait()

    def expert(d, carry):
        layer = (z + d) % sp_count
        for i in range(tp_count):
            e = layer * tp_count + i

            @pl.when(e != me)
            def _():
                go_copy(me, e).wait_recv()

        block = arrived[pl.ds(layer * tp_count, tp_count)].reshape(picks, width)
        gated = dot(block, gate_w[...])
        raised = dot(block, up_w[...])
        hidden = (gated / (1.0 + jnp.exp(-gated)) * raised).astype(BF16)
        done = dot(hidden, down_w[...]).astype(BF16)
        results[pl.ds(layer * tp_count, tp_count)] = done.reshape(tp_count, capacity, width)
        for i in range(tp_count):
            e = layer * tp_count + i

            @pl.when(e != me)
            def _():
                back_copy(e, me).start()

        return carry

    lax.fori_loop(0, sp_count, expert, 0)
    returned[me] = results[me]

    def collect(k, carry):
        e = (me + k) % experts
        back_copy(me, e).wait_recv()
        return carry

    lax.fori_loop(1, experts, collect, 0)
    for q in range(pieces):
        cols = slice(q * piece, (q + 1) * piece)
        back = returned[:, :, cols].reshape(experts * capacity, piece)
        mixed = dot(share_hi[...], back) + dot(share_lo[...], back)
        out[:, cols] = (stream[:, cols].astype(F32) + mixed).astype(BF16)

    @pl.when(z < sp_count - 1)
    def _():
        halo_copy.wait_send()

    for q in range(pieces):
        for k in range(chips):
            pair_copy(k, q).wait_send()
            if k:
                far_copy(k, q).wait_send()

    def flush(k, carry):
        e = (me + k) % experts
        go_copy(e, me).wait_send()
        back_copy(e, me).wait_send()
        return carry

    lax.fori_loop(1, experts, flush, 0)


def fused(
    queries, key_heads, value_heads, sink_logit, out_weight, residual, norm_gain, expert_ids, route_weights,
    gate_weight, up_weight, down_weight,
):
    rows, width = residual.shape
    sp_count, tp_count = lax.axis_size("sp"), lax.axis_size("tp")
    experts = sp_count * tp_count
    top_k = expert_ids.shape[1]
    capacity = max(2, 2 * top_k * rows // experts)
    hidden = gate_weight.shape[2]
    depth = out_weight.shape[0]
    pieces = 4
    chips = tp_count // 2
    part = (chips, pieces, rows, width // pieces)
    box = (experts, capacity, width)
    reach, groups, size = key_heads.shape
    kv = jnp.stack([key_heads, value_heads], 2).reshape(reach, groups * 2 * size)
    vmem = pl.BlockSpec(memory_space=pltpu.VMEM)
    hbm = pl.BlockSpec(memory_space=pl.ANY)
    dma = pltpu.SemaphoreType.DMA
    return pl.pallas_call(
        functools.partial(tail_kernel, (sp_count, tp_count, pieces, capacity)),
        out_shape=jax.ShapeDtypeStruct((rows, width), BF16),
        in_specs=[vmem, vmem, vmem, hbm, vmem, vmem, vmem, vmem, hbm, hbm, hbm],
        out_specs=vmem,
        scratch_shapes=[
            pltpu.VMEM((WINDOW + kv.shape[0], kv.shape[1]), BF16),
            pltpu.VMEM(queries.shape, BF16),
            dma,
            dma,
            pltpu.VMEM((depth, width), BF16),
            pltpu.VMEM((width, hidden), BF16),
            pltpu.VMEM((width, hidden), BF16),
            pltpu.VMEM((hidden, width), BF16),
            pltpu.VMEM(part, BF16),
            pltpu.VMEM(part, BF16),
            pltpu.VMEM(part, BF16),
            pltpu.VMEM(part, BF16),
            pltpu.VMEM((rows, width), BF16),
            pltpu.VMEM((rows, width), BF16),
            pltpu.VMEM((rows, experts * capacity), BF16),
            pltpu.VMEM((rows, experts * capacity), BF16),
            pltpu.VMEM((rows, experts * capacity), BF16),
            pltpu.VMEM(box, BF16),
            pltpu.VMEM(box, BF16),
            pltpu.VMEM(box, BF16),
            pltpu.VMEM(box, BF16),
            dma((4,)),
            dma((chips, pieces)),
            dma((chips, pieces)),
            dma((chips, pieces)),
            dma((chips, pieces)),
            dma((experts,)),
            dma((experts,)),
            dma((experts,)),
            dma((experts,)),
        ],
        compiler_params=pltpu.CompilerParams(
            collective_id=0, has_side_effects=True, vmem_limit_bytes=VMEM_BUDGET
        ),
    )(
        queries, kv, sink_logit[None], out_weight, residual, norm_gain[None], expert_ids.T, route_weights.T,
        gate_weight, up_weight, down_weight,
    )


def on_device(queries, key_heads, value_heads, sink_logit, *rest):
    rows_dev = rest[1].shape[0]
    experts = lax.axis_size("sp") * lax.axis_size("tp")
    fits = 2 * rest[3].shape[1] * rows_dev // experts % 16 == 0 and rows_dev % WINDOW == 0
    if fits:
        return fused(queries, key_heads, value_heads, sink_logit, *rest)
    return tail_plain(attention(queries, key_heads, value_heads, sink_logit), *rest)


def solution(mesh):
    return jax.shard_map(
        on_device,
        mesh=mesh,
        in_specs=(
            P(("grp", "sp"), "tp"),
            P(("grp", "sp"), "tp", None),
            P(("grp", "sp"), "tp", None),
            P("tp"),
            P("tp", None),
            P(("grp", "sp", "tp"), None),
            P(),
            P(("grp", "sp", "tp"), None),
            P(("grp", "sp", "tp"), None),
            P(("sp", "tp"), None, None),
            P(("sp", "tp"), None, None),
            P(("sp", "tp"), None, None),
        ),
        out_specs=P(("grp", "sp", "tp"), None),
        check_vma=False,
    )
```

profile of v0, /device:TPU:31, one launch (start us, length us, event | category | flops | bytes accessed | tf_op | source)
XLA Modules:
  0.0 121.7 jit_solution(12176368414457230718)
XLA Ops:
  0.0 0.9 pad_maximum_fusion
  0.9 0.8 copy.14.kv
  1.6 118.2 %shard_map.118 = bf16[128,2048]{1,0:T(8,128)(2,1)} custom-call(bf16[512,512]{1,0:T(8,128)(2,1)} %queries.1, bf16[512,128]{1,0:T(8,128)(2,1)} %copy.14.kv, f32[1,8]{1,0:T(1,128)} %bitcast.13, bf16[512,2048]{1,0:T(8,128)(2,1)} %out_w_hbm.1, bf16[128,2048]{1,0:T(8,128)(2,1)} %residual.1, f32[1,2048]{1,0:T(1,128)} %bitcast.10, s32[2,128]{1,0:T(2,128)} %bitcast.11, ...), custom_call_target="tpu_custom_call" | custom-call | tf_op jit(solution)/shard_map/pallas_call | solution.py:446
  119.8 1.9 %copy.16 = bf16[128,2048]{1,0:T(8,128)(2,1)} copy(bf16[128,2048]{1,0:T(8,128)(2,1)} %shard_map.118) | data formatting | bytes 1048576
where the time goes:
time: 122 us
  Pallas kernels  118 us (97%)
  local copies, waits for them, and re-layouts  2.64 us (2%)
    pallas_call x1, Pallas kernels, fused(): pl.pallas_call(functools.partial(tail_kernel, (sp_count, tp_count, pieces...  118 us

commit v1 on v0

--- a/solution.py
+++ b/solution.py
@@ -126,12 +126,11 @@
     return (wide + combined).astype(jnp.bfloat16)
 
 
-def routing(ids, weights, experts, capacity):
-    top_k, rows = ids.shape
-    pad = jnp.zeros((-2 * top_k % 8, rows), F32)
-    facts = jnp.concatenate([ids.astype(F32), weights, pad], 0).T
+def routing(facts, first, top_k, experts, capacity):
+    facts = facts.T
+    rows = facts.shape[0]
     ids, weights = facts[:, :top_k], facts[:, top_k : 2 * top_k]
-    expert = lax.broadcasted_iota(jnp.int32, (rows, experts), 1).astype(F32)
+    expert = (first + lax.broadcasted_iota(jnp.int32, (rows, experts), 1)).astype(F32)
     total = jnp.sum(weights, axis=1, keepdims=True)
     member = jnp.zeros((rows, experts), F32)
     share = jnp.zeros((rows, experts), F32)
@@ -156,11 +155,8 @@
     high = share.astype(BF16)
     low = (share - high.astype(F32)).astype(BF16)
     one = jnp.where(taken, 1.0, 0.0)
-    return (
-        one.astype(BF16),
-        (one * dot(high, spread)).astype(BF16),
-        (one * dot(low, spread)).astype(BF16),
-    )
+    shares = jnp.concatenate([one * dot(high, spread), one * dot(low, spread)], 0)
+    return one.T.astype(BF16), shares.astype(BF16)
 
 
 def attend(z, token_rows, queries, sink, seen, attended, at):
@@ -224,6 +220,30 @@
         block(at * (token_rows // window) + b)
 
 
+def plan(m, count, pieces):
+    piece, hop = 1.0 / pieces, 0.15
+    exchange = 0.65
+    mix = 1.25
+
+    def due(s):
+        return abs(s - m)
+
+    steps = []
+    for s in range(count):
+        for q in range(pieces):
+            at = 0.0 if s == m else due(s) - 1 + (q + 1) * piece + hop
+            steps.append((at, "pick", s, q))
+        steps.append((due(s) + exchange, "expert", s, 0))
+        steps.append((due(s) + mix, "mix", s, 0))
+        if s != m and m > 0:
+            origin = 0 if s > m else count - 1
+            for q in range(pieces):
+                at = abs(s - origin) + mix + abs(m - origin) * 0.35 + q * piece
+                steps.append((max(at, due(s) + mix + 0.01), "pass", s, q))
+    steps.sort(key=lambda step: step[0])
+    return [step[1:] for step in steps]
+
+
 def tail_kernel(
     sizes,
     queries, kv, sink, out_w_hbm, residual, gain, ids, weights, gate_hbm, up_hbm, down_hbm,
@@ -231,23 +251,22 @@
     seen, attended, halo_send, halo_recv,
     out_w, gate_w, up_w, down_w,
     pair_out, pair_in, far_out, far_in,
-    stream, normed, slots, share_hi, share_lo,
-    outbox, arrived, results, returned,
+    stream, facts, slots, shares,
+    tokens, outbox, arrived, results, returned,
+    local, total_own, line_out, line_in,
     load_sem, pair_send, pair_recv, far_send, far_recv,
-    go_send, go_recv, back_send, back_recv,
+    facts_send, facts_recv, line_go_send, line_go_recv,
+    go_send, go_recv, back_send, back_recv, line_back_send, line_back_recv,
 ):
     sp_count, tp_count, pieces, capacity = sizes
-    experts = sp_count * tp_count
     chips = tp_count // 2
     z, t = lax.axis_index("sp"), lax.axis_index("tp")
-    me = z * tp_count + t
     x, core = t // 2, t % 2
     other = 1 - core
     rows, width = residual.shape
     piece = width // pieces
-
-    def where(e):
-        return {"sp": e // tp_count, "tp": e % tp_count}
+    top_k = ids.shape[0]
+    picks = tp_count * capacity
 
     loads = [
         pltpu.make_async_copy(src, dst, load_sem.at[i])
@@ -259,15 +278,15 @@
         load.start()
 
     barrier = pltpu.get_barrier_semaphore()
-
-    def greet(k, carry):
+    for k in range(1, sp_count):
         pl.semaphore_signal(
-            barrier, inc=1, device_id=where((me + k) % experts), device_id_type=MESH
-        )
-        return carry
-
-    lax.fori_loop(1, experts, greet, 0)
-    pl.semaphore_wait(barrier, experts - 1)
+            barrier, inc=1, device_id={"sp": (z + k) % sp_count}, device_id_type=MESH
+        )
+    for k in range(1, tp_count):
+        pl.semaphore_signal(
+            barrier, inc=1, device_id={"tp": (t + k) % tp_count}, device_id_type=MESH
+        )
+    pl.semaphore_wait(barrier, sp_count + tp_count - 2)
     reach = kv.shape[0]
     halo_copy = pltpu.make_async_remote_copy(
         kv.at[pl.ds(reach - WINDOW, WINDOW)], seen.at[pl.ds(0, WINDOW)], halo_send, halo_recv,
@@ -278,8 +297,27 @@
     def _():
         halo_copy.start()
 
+    def facts_copy(k):
+        return pltpu.make_async_remote_copy(
+            facts.at[z], facts.at[z], facts_send.at[k], facts_recv.at[z],
+            device_id={"sp": (z + k) % sp_count}, device_id_type=MESH,
+        )
+
+    def facts_wait(s):
+        pltpu.make_async_remote_copy(
+            facts.at[s], facts.at[s], facts_send.at[0], facts_recv.at[s],
+            device_id={"sp": s}, device_id_type=MESH,
+        ).wait_recv()
+
+    pad = jnp.zeros((-2 * top_k % 8, rows), F32)
+    facts[z] = jnp.concatenate([ids[...].astype(F32), weights[...], pad], 0)
+    for k in range(1, sp_count):
+        facts_copy(k).start()
+
     seen[WINDOW:, :] = kv[...]
-    slots[...], share_hi[...], share_lo[...] = routing(ids[...], weights[...], experts, capacity)
+
+    def route(s):
+        slots[s], shares[s] = routing(facts[s], z * tp_count, top_k, tp_count, capacity)
 
     @pl.when(z == 0)
     def _():
@@ -320,6 +358,15 @@
             pair_copy(k, q).wait_recv()
             far_out[k, q] = (mine + pair_in[k, q].astype(F32)).astype(BF16)
             far_copy(k, q).start()
+
+    def route_other(k, carry):
+        s = (z + k) % sp_count
+        facts_wait(s)
+        route(s)
+        return carry
+
+    route(z)
+    lax.fori_loop(1, sp_count, route_other, 0)
     square = jnp.zeros((rows, 1), F32)
     for q in range(pieces):
         cols = slice(q * piece, (q + 1) * piece)
@@ -334,93 +381,148 @@
         value = value.astype(F32)
         square = square + jnp.sum(value * value, axis=1, keepdims=True)
     scale = lax.rsqrt(square / width + EPS)
-    for q in range(pieces):
-        cols = slice(q * piece, (q + 1) * piece)
-        normed[:, cols] = (stream[:, cols].astype(F32) * scale * gain[:, cols]).astype(BF16)
-
-    def go_copy(to, at):
+
+    def line_go(to, s, q, way):
         return pltpu.make_async_remote_copy(
-            outbox.at[to], arrived.at[at], go_send.at[to], go_recv.at[at],
-            device_id=where(to), device_id_type=MESH,
-        )
-
-    def back_copy(to, at):
+            tokens.at[s, q], tokens.at[s, q], line_go_send.at[way, s, q], line_go_recv.at[s, q],
+            device_id={"sp": to}, device_id_type=MESH,
+        )
+
+    def line_back(to, s, q, way):
         return pltpu.make_async_remote_copy(
-            results.at[to], returned.at[at], back_send.at[to], back_recv.at[at],
-            device_id=where(to), device_id_type=MESH,
-        )
-
-    picks = tp_count * capacity
-    for d in range(sp_count):
-        layer = range(d * tp_count, (d + 1) * tp_count)
-        chosen = dot(slots[:, d * picks : (d + 1) * picks], normed[...], ((0,), (0,))).astype(BF16)
-        for i, e in enumerate(layer):
-            outbox[e] = chosen[i * capacity : (i + 1) * capacity]
-
-            @pl.when(e != me)
-            def _():
-                go_copy(e, me).start()
-
-    arrived[me] = outbox[me]
-    for load in loads[1:]:
-        load.wait()
-
-    def expert(d, carry):
-        layer = (z + d) % sp_count
-        for i in range(tp_count):
-            e = layer * tp_count + i
-
-            @pl.when(e != me)
-            def _():
-                go_copy(me, e).wait_recv()
-
-        block = arrived[pl.ds(layer * tp_count, tp_count)].reshape(picks, width)
-        gated = dot(block, gate_w[...])
-        raised = dot(block, up_w[...])
-        hidden = (gated / (1.0 + jnp.exp(-gated)) * raised).astype(BF16)
-        done = dot(hidden, down_w[...]).astype(BF16)
-        results[pl.ds(layer * tp_count, tp_count)] = done.reshape(tp_count, capacity, width)
-        for i in range(tp_count):
-            e = layer * tp_count + i
-
-            @pl.when(e != me)
-            def _():
-                back_copy(e, me).start()
-
-        return carry
-
-    lax.fori_loop(0, sp_count, expert, 0)
-    returned[me] = results[me]
-
-    def collect(k, carry):
-        e = (me + k) % experts
-        back_copy(me, e).wait_recv()
-        return carry
-
-    lax.fori_loop(1, experts, collect, 0)
-    for q in range(pieces):
-        cols = slice(q * piece, (q + 1) * piece)
-        back = returned[:, :, cols].reshape(experts * capacity, piece)
-        mixed = dot(share_hi[...], back) + dot(share_lo[...], back)
-        out[:, cols] = (stream[:, cols].astype(F32) + mixed).astype(BF16)
+            line_out.at[s, q], line_in.at[way, s, q], line_back_send.at[s, q],
+            line_back_recv.at[way, s, q], device_id={"sp": to}, device_id_type=MESH,
+        )
+
+    def go_copy(s, q, to, at):
+        return pltpu.make_async_remote_copy(
+            outbox.at[s, q, to], arrived.at[s, q, at], go_send.at[s, q, to], go_recv.at[s, q, at],
+            device_id={"tp": to}, device_id_type=MESH,
+        )
+
+    def back_copy(s, q, to, at):
+        return pltpu.make_async_remote_copy(
+            results.at[s, q, to], returned.at[s, q, at], back_send.at[s, q, to], back_recv.at[s, q, at],
+            device_id={"tp": to}, device_id_type=MESH,
+        )
+
+    peers = [(t + k) % tp_count for k in range(1, tp_count)]
+    flip = (z * 2 >= sp_count).astype(jnp.int32)
+    place = z + flip * (sp_count - 1 - 2 * z)
+
+    def real(s):
+        return s + flip * (sp_count - 1 - 2 * s)
+
+    def program(m):
+        inner, outer = flip, 1 - flip
+
+        def pick(s, q):
+            r = real(s)
+            if s == m:
+                cols = slice(q * piece, (q + 1) * piece)
+                tokens[r, q] = (stream[:, cols].astype(F32) * scale * gain[:, cols]).astype(BF16)
+                line_go(real(m + 1), r, q, inner).start()
+                if m > 0:
+                    line_go(real(m - 1), r, q, outer).start()
+            else:
+                line_go(r, r, q, inner).wait_recv()
+                if s < m:
+                    line_go(real(m + 1), r, q, inner).start()
+                elif m > 0:
+                    line_go(real(m - 1), r, q, outer).start()
+            chosen = dot(slots[r], tokens[r, q]).astype(BF16)
+            outbox[r, q] = chosen.reshape(tp_count, capacity, piece)
+            for to in peers:
+                go_copy(r, q, to, t).start()
+            arrived[r, q, t] = outbox[r, q, t]
+
+        def expert(s, _):
+            r = real(s)
+            gated = raised = None
+            for q in range(pieces):
+                for peer in peers:
+                    go_copy(r, q, peer, peer).wait_recv()
+                block = arrived[r, q].reshape(picks, piece)
+                part = slice(q * piece, (q + 1) * piece)
+                a, b = dot(block, gate_w[part, :]), dot(block, up_w[part, :])
+                gated, raised = (a, b) if q == 0 else (gated + a, raised + b)
+            hidden = (gated / (1.0 + jnp.exp(-gated)) * raised).astype(BF16)
+            for q in range(pieces):
+                done = dot(hidden, down_w[:, q * piece : (q + 1) * piece]).astype(BF16)
+                results[r, q] = done.reshape(tp_count, capacity, piece)
+                for to in peers:
+                    back_copy(r, q, to, t).start()
+                returned[r, q, t] = results[r, q, t]
+
+        def mix(s, _):
+            r = real(s)
+            for q in range(pieces):
+                for peer in peers:
+                    back_copy(r, q, peer, peer).wait_recv()
+                both = dot(shares[r], returned[r, q].reshape(picks, piece))
+                mixed = both[:rows] + both[rows:]
+                if s == m:
+                    total_own[q] = stream[:, q * piece : (q + 1) * piece].astype(F32) + mixed
+                elif m == 0:
+                    line_out[r, q] = mixed.astype(BF16)
+                    line_back(real(1), r, q, inner).start()
+                else:
+                    local[r, q] = mixed
+
+        def hand_on(s, q):
+            r = real(s)
+            way, to = (inner, m + 1) if s > m else (outer, m - 1)
+            line_back(real(to), r, q, way).wait_recv()
+            line_out[r, q] = (local[r, q] + line_in[way, r, q].astype(F32)).astype(BF16)
+            line_back(real(to), r, q, way).start()
+
+        act = {"pick": pick, "expert": expert, "mix": mix, "pass": hand_on}
+        loaded = False
+        for name, s, q in plan(m, sp_count, pieces):
+            if name == "expert" and not loaded:
+                loaded = True
+                for load in loads[1:]:
+                    load.wait()
+            act[name](s, q)
+        for q in range(pieces):
+            total = total_own[q]
+            for way in [inner, outer] if m > 0 else [outer]:
+                line_back(real(m + 1), z, q, way).wait_recv()
+                total = total + line_in[way, z, q].astype(F32)
+            out[:, q * piece : (q + 1) * piece] = total.astype(BF16)
+        for s in range(sp_count):
+            for q in range(pieces):
+                r = real(s)
+                if s <= m:
+                    line_go(real(m + 1), r, q, inner).wait_send()
+                if s >= m and m > 0:
+                    line_go(real(m - 1), r, q, outer).wait_send()
+                if s != m:
+                    line_back(real(m + 1), r, q, inner).wait_send()
+
+    for m in range((sp_count + 1) // 2):
+        pl.when(place == m)(functools.partial(program, m))
 
     @pl.when(z < sp_count - 1)
     def _():
         halo_copy.wait_send()
 
+    for k in range(1, sp_count):
+        facts_copy(k).wait_send()
     for q in range(pieces):
         for k in range(chips):
             pair_copy(k, q).wait_send()
             if k:
                 far_copy(k, q).wait_send()
 
-    def flush(k, carry):
-        e = (me + k) % experts
-        go_copy(e, me).wait_send()
-        back_copy(e, me).wait_send()
+    def flush(i, carry):
+        s, q = i // pieces, i % pieces
+        for peer in peers:
+            go_copy(s, q, peer, t).wait_send()
+            back_copy(s, q, peer, t).wait_send()
         return carry
 
-    lax.fori_loop(1, experts, flush, 0)
+    lax.fori_loop(0, sp_count * pieces, flush, 0)
 
 
 def fused(
@@ -436,8 +538,11 @@
     depth = out_weight.shape[0]
     pieces = 4
     chips = tp_count // 2
-    part = (chips, pieces, rows, width // pieces)
-    box = (experts, capacity, width)
+    piece = width // pieces
+    part = (chips, pieces, rows, piece)
+    line = (sp_count, pieces, rows, piece)
+    box = (sp_count, pieces, tp_count, capacity, piece)
+    picks = tp_count * capacity
     reach, groups, size = key_heads.shape
     kv = jnp.stack([key_heads, value_heads], 2).reshape(reach, groups * 2 * size)
     vmem = pl.BlockSpec(memory_space=pltpu.VMEM)
@@ -462,23 +567,33 @@
             pltpu.VMEM(part, BF16),
             pltpu.VMEM(part, BF16),
             pltpu.VMEM((rows, width), BF16),
-            pltpu.VMEM((rows, width), BF16),
-            pltpu.VMEM((rows, experts * capacity), BF16),
-            pltpu.VMEM((rows, experts * capacity), BF16),
-            pltpu.VMEM((rows, experts * capacity), BF16),
+            pltpu.VMEM((sp_count, 2 * top_k + -2 * top_k % 8, rows), F32),
+            pltpu.VMEM((sp_count, picks, rows), BF16),
+            pltpu.VMEM((sp_count, 2 * rows, picks), BF16),
+            pltpu.VMEM(line, BF16),
             pltpu.VMEM(box, BF16),
             pltpu.VMEM(box, BF16),
             pltpu.VMEM(box, BF16),
             pltpu.VMEM(box, BF16),
+            pltpu.VMEM(line, F32),
+            pltpu.VMEM(line[1:], F32),
+            pltpu.VMEM(line, BF16),
+            pltpu.VMEM((2,) + line, BF16),
             dma((4,)),
             dma((chips, pieces)),
             dma((chips, pieces)),
             dma((chips, pieces)),
             dma((chips, pieces)),
-            dma((experts,)),
-            dma((experts,)),
-            dma((experts,)),
-            dma((experts,)),
+            dma((sp_count,)),
+            dma((sp_count,)),
+            dma((2, sp_count, pieces)),
+            dma((sp_count, pieces)),
+            dma((sp_count, pieces, tp_count)),
+            dma((sp_count, pieces, tp_count)),
+            dma((sp_count, pieces, tp_count)),
+            dma((sp_count, pieces, tp_count)),
+            dma((sp_count, pieces)),
+            dma((2, sp_count, pieces)),
         ],
         compiler_params=pltpu.CompilerParams(
             collective_id=0, has_side_effects=True, vmem_limit_bytes=VMEM_BUDGET
@@ -493,6 +608,7 @@
     rows_dev = rest[1].shape[0]
     experts = lax.axis_size("sp") * lax.axis_size("tp")
     fits = 2 * rest[3].shape[1] * rows_dev // experts % 16 == 0 and rows_dev % WINDOW == 0
+    fits = fits and lax.axis_size("sp") > 1
     if fits:
         return fused(queries, key_heads, value_heads, sink_logit, *rest)
     return tail_plain(attention(queries, key_heads, value_heads, sink_logit), *rest)

time: 122 us -> 113 us (0.926)
  the two profiles are of different devices: /device:TPU:31 before, /device:TPU:0 now
where the time goes in v1:
time: 113 us; the launch traced here: 112 us
  Pallas kernels  109 us (96%)
  local copies, waits for them, and re-layouts  2.64 us (2%)
    pallas_call x1, Pallas kernels, fused(): pl.pallas_call(functools.partial(tail_kernel, (sp_count, tp_count, pieces...  109 us

profile of v1, /device:TPU:0, one launch (start us, length us, event | category | flops | bytes accessed | tf_op | source)
XLA Modules:
  0.0 112.4 jit_solution(12343108314449294369)
XLA Ops:
  0.0 0.9 pad_maximum_fusion
  0.9 0.8 copy.14.kv
  1.6 108.9 %shard_map.118 = bf16[128,2048]{1,0:T(8,128)(2,1)} custom-call(bf16[512,512]{1,0:T(8,128)(2,1)} %queries.1, bf16[512,128]{1,0:T(8,128)(2,1)} %copy.14.kv, f32[1,8]{1,0:T(1,128)} %bitcast.13, bf16[512,2048]{1,0:T(8,128)(2,1)} %out_w_hbm.1, bf16[128,2048]{1,0:T(8,128)(2,1)} %residual.1, f32[1,2048]{1,0:T(1,128)} %bitcast.10, s32[2,128]{1,0:T(2,128)} %bitcast.11, ...), custom_call_target="tpu_custom_call" | custom-call | tf_op jit(solution)/shard_map/pallas_call | solution.py:551
  110.6 1.9 %copy.16 = bf16[128,2048]{1,0:T(8,128)(2,1)} copy(bf16[128,2048]{1,0:T(8,128)(2,1)} %shard_map.118) | data formatting | bytes 1048576

commit v2 on v1

--- a/solution.py
+++ b/solution.py
@@ -220,35 +220,97 @@
         block(at * (token_rows // window) + b)
 
 
-def plan(m, count, pieces):
-    piece, hop = 1.0 / pieces, 0.15
-    exchange = 0.65
-    mix = 1.25
-
-    def due(s):
-        return abs(s - m)
-
-    steps = []
-    for s in range(count):
-        for q in range(pieces):
-            at = 0.0 if s == m else due(s) - 1 + (q + 1) * piece + hop
-            steps.append((at, "pick", s, q))
-        steps.append((due(s) + exchange, "expert", s, 0))
-        steps.append((due(s) + mix, "mix", s, 0))
-        if s != m and m > 0:
-            origin = 0 if s > m else count - 1
-            for q in range(pieces):
-                at = abs(s - origin) + mix + abs(m - origin) * 0.35 + q * piece
-                steps.append((max(at, due(s) + mix + 0.01), "pass", s, q))
-    steps.sort(key=lambda step: step[0])
-    return [step[1:] for step in steps]
+def timeline(count, pieces, favour=None):
+    hop, narrow, tick = 0.6, 0.5, 0.05
+    line_lead, layer_lead = 0.3, 0.6
+    cost = {"pick": 0.07, "expert": 0.67, "mix": 0.08, "pass": 0.02, "norm": 0.02}
+    every = range(count)
+    parts = [(s, q) for s in every for q in range(pieces)]
+    landed = {(d, d, q): 0.0 for d in every for q in range(pieces)}
+    came, back, mixed, handed = {}, {}, {}, {}
+    line, layer, busy = {}, [0.0] * count, [0.0] * count
+    done = [set() for _ in every]
+    steps = [[("norm", d, q) for q in range(pieces)] for d in every]
+    now = 0.0
+
+    def put(d, way, at, board, part):
+        line[d, way] = max(line.get((d, way), 0.0), at) + 1
+        board[(d + way,) + part] = line[d, way] + hop
+
+    def there(board, d, part):
+        return board.get((d,) + part, now + 1) <= now
+
+    def choose(d):
+        for way, name in ((-1, "send_out"), (1, "send_in")):
+            if 0 <= d + way < count and line.get((d, way), 0.0) <= now + line_lead:
+                ready = [
+                    p
+                    for p in parts
+                    if (p[0] - d) * way <= 0 and there(landed, d, p) and (name, p) not in done[d]
+                ]
+                if ready:
+                    return name, min(ready, key=lambda p: (-abs(p[0] - d), p[1]))
+        ready = [
+            p
+            for p in parts
+            if p[0] != d and there(handed, d, p) and there(mixed, d, p) and ("pass", p) not in done[d]
+        ]
+        if ready:
+            return "pass", min(ready, key=lambda p: handed[(d,) + p])
+        for p in parts:
+            if there(back, d, p) and ("mix", p) not in done[d]:
+                return "mix", p
+        ready = [
+            (s, 0)
+            for s in every
+            if there(came, d, (s, pieces - 1)) and ("expert", (s, 0)) not in done[d]
+        ]
+        if ready:
+            return "expert", min(ready, key=lambda p: came[d, p[0], pieces - 1])
+        ready = [p for p in parts if there(landed, d, p) and ("pick", p) not in done[d]]
+        if ready and layer[d] <= now + layer_lead:
+            return "pick", min(ready, key=lambda p: (favour[d][p[0]] if favour else 0, p))
+        return None
+
+    size = count * pieces
+    due = [{"mix": size, "pass": size - pieces if 0 < d < count - 1 else 0} for d in every]
+    while any(sum(k == name for k, _ in done[d]) < due[d][name] for d in every for name in due[d]):
+        for d in every:
+            while busy[d] <= now:
+                step = choose(d)
+                if step is None:
+                    break
+                name, part = step
+                done[d].add(step)
+                steps[d].append((name,) + part)
+                busy[d] = now + cost.get(name, 0.0)
+                if name == "send_in":
+                    put(d, 1, now, landed, part)
+                elif name == "send_out":
+                    put(d, -1, now, landed, part)
+                elif name == "pick":
+                    layer[d] = max(layer[d], busy[d]) + narrow
+                    came[(d,) + part] = layer[d] + hop
+                elif name == "expert":
+                    for q in range(pieces):
+                        ready = now + cost[name] * (q + 3) / (pieces + 2)
+                        layer[d] = max(layer[d], ready) + narrow
+                        back[d, part[0], q] = layer[d] + hop
+                elif name == "mix":
+                    mixed[(d,) + part] = busy[d]
+                if name == "pass" or (name == "mix" and part[0] != d and d in (0, count - 1)):
+                    put(d, 1 if part[0] > d else -1, busy[d], handed, part)
+        now += tick
+    if favour is None:
+        return timeline(count, pieces, [[landed[d, s, pieces - 1] for s in every] for d in every])
+    return steps
 
 
 def tail_kernel(
     sizes,
-    queries, kv, sink, out_w_hbm, residual, gain, ids, weights, gate_hbm, up_hbm, down_hbm,
+    queries_hbm, keys, values, sink, out_w_hbm, residual_hbm, gain, ids, weights, gate_hbm, up_hbm, down_hbm,
     out,
-    seen, attended, halo_send, halo_recv,
+    queries, residual, seen, attended, halo_send, halo_recv,
     out_w, gate_w, up_w, down_w,
     pair_out, pair_in, far_out, far_in,
     stream, facts, slots, shares,
@@ -263,19 +325,10 @@
     z, t = lax.axis_index("sp"), lax.axis_index("tp")
     x, core = t // 2, t % 2
     other = 1 - core
-    rows, width = residual.shape
+    rows, width = residual_hbm.shape
     piece = width // pieces
     top_k = ids.shape[0]
     picks = tp_count * capacity
-
-    loads = [
-        pltpu.make_async_copy(src, dst, load_sem.at[i])
-        for i, (src, dst) in enumerate(
-            ((out_w_hbm, out_w), (gate_hbm.at[0], gate_w), (up_hbm.at[0], up_w), (down_hbm.at[0], down_w))
-        )
-    ]
-    for load in loads:
-        load.start()
 
     barrier = pltpu.get_barrier_semaphore()
     for k in range(1, sp_count):
@@ -286,10 +339,32 @@
         pl.semaphore_signal(
             barrier, inc=1, device_id={"tp": (t + k) % tp_count}, device_id_type=MESH
         )
+    loads = [
+        pltpu.make_async_copy(src, dst, load_sem.at[i])
+        for i, (src, dst) in enumerate(
+            (
+                (queries_hbm, queries), (out_w_hbm, out_w), (residual_hbm, residual),
+                (gate_hbm.at[0], gate_w), (up_hbm.at[0], up_w), (down_hbm.at[0], down_w),
+            )
+        )
+    ]
+    for load in loads:
+        load.start()
+
+    groups, size, reach = keys.shape
+    for g in range(groups):
+        both = jnp.concatenate([keys[g], values[g]], 0)
+        seen[WINDOW:, 2 * g * size : (2 * g + 2) * size] = both.T
+
+    @pl.when(z == 0)
+    def _():
+        seen[:WINDOW, :] = jnp.zeros((WINDOW, seen.shape[1]), BF16)
+
+    pad = jnp.zeros((-2 * top_k % 8, rows), F32)
+    facts[z] = jnp.concatenate([ids[...].astype(F32), weights[...], pad], 0)
     pl.semaphore_wait(barrier, sp_count + tp_count - 2)
-    reach = kv.shape[0]
     halo_copy = pltpu.make_async_remote_copy(
-        kv.at[pl.ds(reach - WINDOW, WINDOW)], seen.at[pl.ds(0, WINDOW)], halo_send, halo_recv,
+        seen.at[pl.ds(reach, WINDOW)], seen.at[pl.ds(0, WINDOW)], halo_send, halo_recv,
         device_id={"sp": jnp.minimum(z + 1, sp_count - 1)}, device_id_type=MESH,
     )
 
@@ -299,35 +374,30 @@
 
     def facts_copy(k):
         return pltpu.make_async_remote_copy(
-            facts.at[z], facts.at[z], facts_send.at[k], facts_recv.at[z],
+            facts.at[z], facts.at[z], facts_send, facts_recv.at[z],
             device_id={"sp": (z + k) % sp_count}, device_id_type=MESH,
         )
 
     def facts_wait(s):
         pltpu.make_async_remote_copy(
-            facts.at[s], facts.at[s], facts_send.at[0], facts_recv.at[s],
+            facts.at[s], facts.at[s], facts_send, facts_recv.at[s],
             device_id={"sp": s}, device_id_type=MESH,
         ).wait_recv()
 
-    pad = jnp.zeros((-2 * top_k % 8, rows), F32)
-    facts[z] = jnp.concatenate([ids[...].astype(F32), weights[...], pad], 0)
     for k in range(1, sp_count):
         facts_copy(k).start()
 
-    seen[WINDOW:, :] = kv[...]
-
     def route(s):
         slots[s], shares[s] = routing(facts[s], z * tp_count, top_k, tp_count, capacity)
 
-    @pl.when(z == 0)
-    def _():
-        seen[:WINDOW, :] = jnp.zeros((WINDOW, kv.shape[1]), BF16)
-
-    @pl.when(z > 0)
-    def _():
-        halo_copy.wait_recv()
-
     loads[0].wait()
+
+    def attend_block(at):
+        @pl.when((z > 0) & (at == 0))
+        def _():
+            halo_copy.wait_recv()
+
+        attend(z, rows, queries, sink, seen, attended, at)
 
     def partial(chip, which, q):
         block = attended[pl.ds(pl.multiple_of((chip * 2 + which) * rows, rows), rows), :]
@@ -335,24 +405,26 @@
 
     def pair_copy(k, q):
         return pltpu.make_async_remote_copy(
-            pair_out.at[k, q], pair_in.at[k, q], pair_send.at[k, q], pair_recv.at[k, q],
+            pair_out.at[k, q], pair_in.at[k, q], pair_send, pair_recv.at[k, q],
             device_id={"tp": x * 2 + other}, device_id_type=MESH,
         )
 
     def far_copy(k, q):
         return pltpu.make_async_remote_copy(
-            far_out.at[k, q], far_in.at[k, q], far_send.at[k, q], far_recv.at[k, q],
+            far_out.at[k, q], far_in.at[k, q], far_send, far_recv.at[k, q],
             device_id={"tp": ((x + k) % chips) * 2 + core}, device_id_type=MESH,
         )
 
     order = list(range(1, chips)) + [0]
     for k in order:
         chip = (x + k) % chips
-        attend(z, rows, queries, sink, seen, attended, chip * 2 + other)
+        attend_block(chip * 2 + other)
+        if k == order[0]:
+            loads[1].wait()
         for q in range(pieces):
             pair_out[k, q] = partial(chip, other, q).astype(BF16)
             pair_copy(k, q).start()
-        attend(z, rows, queries, sink, seen, attended, chip * 2 + core)
+        attend_block(chip * 2 + core)
         for q in range(pieces if k else 0):
             mine = partial(chip, core, q)
             pair_copy(k, q).wait_recv()
@@ -366,6 +438,7 @@
         return carry
 
     route(z)
+    loads[2].wait()
     lax.fori_loop(1, sp_count, route_other, 0)
     square = jnp.zeros((rows, 1), F32)
     for q in range(pieces):
@@ -382,29 +455,41 @@
         square = square + jnp.sum(value * value, axis=1, keepdims=True)
     scale = lax.rsqrt(square / width + EPS)
 
-    def line_go(to, s, q, way):
+    def line_go(to, s, q):
         return pltpu.make_async_remote_copy(
-            tokens.at[s, q], tokens.at[s, q], line_go_send.at[way, s, q], line_go_recv.at[s, q],
+            tokens.at[s, q], tokens.at[s, q], line_go_send, line_go_recv.at[s, q],
             device_id={"sp": to}, device_id_type=MESH,
         )
 
     def line_back(to, s, q, way):
         return pltpu.make_async_remote_copy(
-            line_out.at[s, q], line_in.at[way, s, q], line_back_send.at[s, q],
+            line_out.at[s, q], line_in.at[way, s, q], line_back_send,
             line_back_recv.at[way, s, q], device_id={"sp": to}, device_id_type=MESH,
         )
 
     def go_copy(s, q, to, at):
         return pltpu.make_async_remote_copy(
-            outbox.at[s, q, to], arrived.at[s, q, at], go_send.at[s, q, to], go_recv.at[s, q, at],
+            outbox.at[s, q, to], arrived.at[s, q, at], go_send, go_recv.at[s, q],
             device_id={"tp": to}, device_id_type=MESH,
         )
 
     def back_copy(s, q, to, at):
         return pltpu.make_async_remote_copy(
-            results.at[s, q, to], returned.at[s, q, at], back_send.at[s, q, to], back_recv.at[s, q, at],
+            results.at[s, q, to], returned.at[s, q, at], back_send, back_recv.at[s, q],
             device_id={"tp": to}, device_id_type=MESH,
         )
+
+    def box_wait(box, send, recv, s, q):
+        part = pl.ds(0, tp_count - 1)
+        pltpu.make_async_remote_copy(
+            box.at[s, q, part], box.at[s, q, part], send, recv.at[s, q],
+            device_id={"tp": (t + 1) % tp_count}, device_id_type=MESH,
+        ).wait_recv()
+
+    def sent(ref, send, peer):
+        pltpu.make_async_remote_copy(
+            ref, ref, send, halo_recv, device_id=peer, device_id_type=MESH
+        ).wait_send()
 
     peers = [(t + k) % tp_count for k in range(1, tp_count)]
     flip = (z * 2 >= sp_count).astype(jnp.int32)
@@ -416,20 +501,21 @@
     def program(m):
         inner, outer = flip, 1 - flip
 
+        def norm(s, q):
+            cols = slice(q * piece, (q + 1) * piece)
+            tokens[z, q] = (stream[:, cols].astype(F32) * scale * gain[:, cols]).astype(BF16)
+
+        def land(s, q):
+            line_go(real(s), real(s), q).wait_recv()
+
+        def send_in(s, q):
+            line_go(real(m + 1), real(s), q).start()
+
+        def send_out(s, q):
+            line_go(real(m - 1), real(s), q).start()
+
         def pick(s, q):
             r = real(s)
-            if s == m:
-                cols = slice(q * piece, (q + 1) * piece)
-                tokens[r, q] = (stream[:, cols].astype(F32) * scale * gain[:, cols]).astype(BF16)
-                line_go(real(m + 1), r, q, inner).start()
-                if m > 0:
-                    line_go(real(m - 1), r, q, outer).start()
-            else:
-                line_go(r, r, q, inner).wait_recv()
-                if s < m:
-                    line_go(real(m + 1), r, q, inner).start()
-                elif m > 0:
-                    line_go(real(m - 1), r, q, outer).start()
             chosen = dot(slots[r], tokens[r, q]).astype(BF16)
             outbox[r, q] = chosen.reshape(tp_count, capacity, piece)
             for to in peers:
@@ -440,8 +526,7 @@
             r = real(s)
             gated = raised = None
             for q in range(pieces):
-                for peer in peers:
-                    go_copy(r, q, peer, peer).wait_recv()
+                box_wait(arrived, go_send, go_recv, r, q)
                 block = arrived[r, q].reshape(picks, piece)
                 part = slice(q * piece, (q + 1) * piece)
                 a, b = dot(block, gate_w[part, :]), dot(block, up_w[part, :])
@@ -454,20 +539,18 @@
                     back_copy(r, q, to, t).start()
                 returned[r, q, t] = results[r, q, t]
 
-        def mix(s, _):
+        def mix(s, q):
             r = real(s)
-            for q in range(pieces):
-                for peer in peers:
-                    back_copy(r, q, peer, peer).wait_recv()
-                both = dot(shares[r], returned[r, q].reshape(picks, piece))
-                mixed = both[:rows] + both[rows:]
-                if s == m:
-                    total_own[q] = stream[:, q * piece : (q + 1) * piece].astype(F32) + mixed
-                elif m == 0:
-                    line_out[r, q] = mixed.astype(BF16)
-                    line_back(real(1), r, q, inner).start()
-                else:
-                    local[r, q] = mixed
+            box_wait(returned, back_send, back_recv, r, q)
+            both = dot(shares[r], returned[r, q].reshape(picks, piece))
+            mixed = both[:rows] + both[rows:]
+            if s == m:
+                total_own[q] = stream[:, q * piece : (q + 1) * piece].astype(F32) + mixed
+            elif m == 0:
+                line_out[r, q] = mixed.astype(BF16)
+                line_back(real(1), r, q, inner).start()
+            else:
+                local[r, q] = mixed
 
         def hand_on(s, q):
             r = real(s)
@@ -476,13 +559,19 @@
             line_out[r, q] = (local[r, q] + line_in[way, r, q].astype(F32)).astype(BF16)
             line_back(real(to), r, q, way).start()
 
-        act = {"pick": pick, "expert": expert, "mix": mix, "pass": hand_on}
-        loaded = False
-        for name, s, q in plan(m, sp_count, pieces):
-            if name == "expert" and not loaded:
-                loaded = True
-                for load in loads[1:]:
+        act = {
+            "norm": norm, "send_in": send_in, "send_out": send_out,
+            "pick": pick, "expert": expert, "mix": mix, "pass": hand_on,
+        }
+        waited = set()
+        for name, s, q in steps[m]:
+            if name == "expert" and "loads" not in waited:
+                waited.add("loads")
+                for load in loads[3:]:
                     load.wait()
+            if name in ("pick", "send_in", "send_out") and s != m and (s, q) not in waited:
+                waited.add((s, q))
+                land(s, q)
             act[name](s, q)
         for q in range(pieces):
             total = total_own[q]
@@ -490,16 +579,12 @@
                 line_back(real(m + 1), z, q, way).wait_recv()
                 total = total + line_in[way, z, q].astype(F32)
             out[:, q * piece : (q + 1) * piece] = total.astype(BF16)
-        for s in range(sp_count):
-            for q in range(pieces):
-                r = real(s)
-                if s <= m:
-                    line_go(real(m + 1), r, q, inner).wait_send()
-                if s >= m and m > 0:
-                    line_go(real(m - 1), r, q, outer).wait_send()
-                if s != m:
-                    line_back(real(m + 1), r, q, inner).wait_send()
-
+        peer = {"sp": real(m + 1)}
+        for _ in range(sp_count + 1 if m > 0 else 1):
+            sent(tokens.at[0], line_go_send, peer)
+        sent(line_out.at[pl.ds(0, sp_count - 1)], line_back_send, peer)
+
+    steps = timeline(sp_count, pieces)
     for m in range((sp_count + 1) // 2):
         pl.when(place == m)(functools.partial(program, m))
 
@@ -507,22 +592,12 @@
     def _():
         halo_copy.wait_send()
 
-    for k in range(1, sp_count):
-        facts_copy(k).wait_send()
-    for q in range(pieces):
-        for k in range(chips):
-            pair_copy(k, q).wait_send()
-            if k:
-                far_copy(k, q).wait_send()
-
-    def flush(i, carry):
-        s, q = i // pieces, i % pieces
-        for peer in peers:
-            go_copy(s, q, peer, t).wait_send()
-            back_copy(s, q, peer, t).wait_send()
-        return carry
-
-    lax.fori_loop(0, sp_count * pieces, flush, 0)
+    peer = {"tp": x * 2 + other}
+    sent(facts.at[pl.ds(0, sp_count - 1)], facts_send, {"sp": (z + 1) % sp_count})
+    sent(pair_out, pair_send, peer)
+    sent(far_out.at[pl.ds(1, chips - 1)], far_send, peer)
+    sent(outbox.at[:, :, pl.ds(0, tp_count - 1)], go_send, peer)
+    sent(results.at[:, :, pl.ds(0, tp_count - 1)], back_send, peer)
 
 
 def fused(
@@ -544,17 +619,19 @@
     box = (sp_count, pieces, tp_count, capacity, piece)
     picks = tp_count * capacity
     reach, groups, size = key_heads.shape
-    kv = jnp.stack([key_heads, value_heads], 2).reshape(reach, groups * 2 * size)
+    keys, values = key_heads.transpose(1, 2, 0), value_heads.transpose(1, 2, 0)
     vmem = pl.BlockSpec(memory_space=pltpu.VMEM)
     hbm = pl.BlockSpec(memory_space=pl.ANY)
     dma = pltpu.SemaphoreType.DMA
     return pl.pallas_call(
         functools.partial(tail_kernel, (sp_count, tp_count, pieces, capacity)),
         out_shape=jax.ShapeDtypeStruct((rows, width), BF16),
-        in_specs=[vmem, vmem, vmem, hbm, vmem, vmem, vmem, vmem, hbm, hbm, hbm],
+        in_specs=[hbm, vmem, vmem, vmem, hbm, hbm, vmem, vmem, vmem, hbm, hbm, hbm],
         out_specs=vmem,
         scratch_shapes=[
-            pltpu.VMEM((WINDOW + kv.shape[0], kv.shape[1]), BF16),
+            pltpu.VMEM(queries.shape, BF16),
+            pltpu.VMEM(residual.shape, BF16),
+            pltpu.VMEM((WINDOW + reach, groups * 2 * size), BF16),
             pltpu.VMEM(queries.shape, BF16),
             dma,
             dma,
@@ -579,27 +656,27 @@
             pltpu.VMEM(line[1:], F32),
             pltpu.VMEM(line, BF16),
             pltpu.VMEM((2,) + line, BF16),
-            dma((4,)),
+            dma((6,)),
+            dma,
             dma((chips, pieces)),
+            dma,
             dma((chips, pieces)),
-            dma((chips, pieces)),
-            dma((chips, pieces)),
+            dma,
             dma((sp_count,)),
-            dma((sp_count,)),
-            dma((2, sp_count, pieces)),
+            dma,
             dma((sp_count, pieces)),
-            dma((sp_count, pieces, tp_count)),
-            dma((sp_count, pieces, tp_count)),
-            dma((sp_count, pieces, tp_count)),
-            dma((sp_count, pieces, tp_count)),
+            dma,
             dma((sp_count, pieces)),
+            dma,
+            dma((sp_count, pieces)),
+            dma,
             dma((2, sp_count, pieces)),
         ],
         compiler_params=pltpu.CompilerParams(
             collective_id=0, has_side_effects=True, vmem_limit_bytes=VMEM_BUDGET
         ),
     )(
-        queries, kv, sink_logit[None], out_weight, residual, norm_gain[None], expert_ids.T, route_weights.T,
+        queries, keys, values, sink_logit[None], out_weight, residual, norm_gain[None], expert_ids.T, route_weights.T,
         gate_weight, up_weight, down_weight,
     )
 
@@ -608,7 +685,7 @@
     rows_dev = rest[1].shape[0]
     experts = lax.axis_size("sp") * lax.axis_size("tp")
     fits = 2 * rest[3].shape[1] * rows_dev // experts % 16 == 0 and rows_dev % WINDOW == 0
-    fits = fits and lax.axis_size("sp") > 1
+    fits = fits and lax.axis_size("sp") > 1 and lax.axis_size("tp") > 2
     if fits:
         return fused(queries, key_heads, value_heads, sink_logit, *rest)
     return tail_plain(attention(queries, key_heads, value_heads, sink_logit), *rest)

time: 113 us -> 95.6 us (0.85)
  Pallas kernels: 109 us -> 93.5 us
    pallas_call x1, Pallas kernels: 109 us -> 93.5 us  [fused(): pl.pallas_call(functools.partial(tail_kernel, (sp_count, tp_count, pieces...]
where the time goes in v2:
time: 95.6 us; the launch traced here: 95.4 us
  Pallas kernels  93.5 us (98%)
  local copies, waits for them, and re-layouts  1.88 us (2%)
    pallas_call x1, Pallas kernels, fused(): pl.pallas_call(functools.partial(tail_kernel, (sp_count, tp_count, pieces...  93.5 us

profile of v2, /device:TPU:0, one launch (start us, length us, event | category | flops | bytes accessed | tf_op | source)
XLA Modules:
  0.0 95.4 jit_solution(8511708527555782937)
XLA Ops:
  0.0 93.5 %shard_map.118 = bf16[128,2048]{1,0:T(8,128)(2,1)} custom-call(bf16[512,512]{1,0:T(8,128)(2,1)} %queries_hbm.1, bf16[1,64,512]{2,1,0:T(8,128)(2,1)} %bitcast.6, bf16[1,64,512]{2,1,0:T(8,128)(2,1)} %bitcast.7, f32[1,8]{1,0:T(1,128)} %bitcast.11, bf16[512,2048]{1,0:T(8,128)(2,1)} %out_w_hbm.1, bf16[128,2048]{1,0:T(8,128)(2,1)} %residual_hbm.1, ...), custom_call_target="tpu_custom_call" | custom-call | tf_op jit(solution)/shard_map/pallas_call | solution.py:626
  93.6 1.9 %copy.14 = bf16[128,2048]{1,0:T(8,128)(2,1)} copy(bf16[128,2048]{1,0:T(8,128)(2,1)} %shard_map.118) | data formatting | bytes 1048576

commit v3 on v2

--- a/solution.py
+++ b/solution.py
@@ -159,7 +159,7 @@
     return one.T.astype(BF16), shares.astype(BF16)
 
 
-def attend(z, token_rows, queries, sink, seen, attended, at):
+def attend(z, queries, sink, seen, attended, first, count):
     window = WINDOW
     rows, lanes = queries.shape[0], seen.shape[1]
     heads = sink.shape[1]
@@ -167,89 +167,90 @@
     groups = lanes // (2 * size)
     share = heads // groups
     pairs = share // 2
-    tall = pairs * window
-    query = lax.broadcasted_iota(jnp.int32, (tall, 2 * window), 0) % window
-    key = lax.broadcasted_iota(jnp.int32, (tall, 2 * window), 1)
+    tall, reach = pairs * count, window + count
+    query = lax.broadcasted_iota(jnp.int32, (tall, reach), 0) % count
+    key = lax.broadcasted_iota(jnp.int32, (tall, reach), 1)
     distance = query + window - key
-    band = (distance >= 0) & (distance < window)
-
-    def block(b):
-        allowed = band & ((z * rows + b * window - window) + key >= 0)
-        span = seen[pl.ds(pl.multiple_of(b * window, window), 2 * window), :]
-        here = pl.ds(pl.multiple_of(b * window, window), window)
-        for g in range(groups):
-            keys = span[:, 2 * g * size : (2 * g + 1) * size]
-            values = span[:, (2 * g + 1) * size : (2 * g + 2) * size]
-            none, ones = jnp.zeros_like(keys), jnp.ones_like(values)
-            wide = jnp.concatenate(
+    allowed = (distance >= 0) & (distance < window) & ((z * rows + first - window) + key >= 0)
+    span = seen[pl.ds(pl.multiple_of(first, count), reach), :]
+    here = pl.ds(pl.multiple_of(first, count), count)
+    for g in range(groups):
+        keys = span[:, 2 * g * size : (2 * g + 1) * size]
+        values = span[:, (2 * g + 1) * size : (2 * g + 2) * size]
+        none, ones = jnp.zeros_like(keys), jnp.ones_like(values)
+        wide = jnp.concatenate(
+            [
+                queries[here, (g * share + 2 * i) * size : (g * share + 2 * i + 2) * size]
+                for i in range(pairs)
+            ],
+            0,
+        )
+        sides = []
+        for odd in range(2):
+            two_keys = jnp.concatenate([none, keys] if odd else [keys, none], 1)
+            two_values = jnp.concatenate([ones, values] if odd else [values, ones], 1)
+            score = dot(wide, two_keys, ((1,), (1,))) * size**-0.5
+            score = jnp.where(allowed, score, -1e30)
+            drain = jnp.concatenate(
                 [
-                    queries[here, (g * share + 2 * i) * size : (g * share + 2 * i + 2) * size]
+                    jnp.broadcast_to(
+                        sink[0:1, g * share + 2 * i + odd : g * share + 2 * i + odd + 1],
+                        (count, 1),
+                    )
                     for i in range(pairs)
                 ],
                 0,
             )
-            sides = []
-            for odd in range(2):
-                two_keys = jnp.concatenate([none, keys] if odd else [keys, none], 1)
-                two_values = jnp.concatenate([ones, values] if odd else [values, ones], 1)
-                score = dot(wide, two_keys, ((1,), (1,))) * size**-0.5
-                score = jnp.where(allowed, score, -1e30)
-                drain = jnp.concatenate(
-                    [
-                        jnp.broadcast_to(
-                            sink[0:1, g * share + 2 * i + odd : g * share + 2 * i + odd + 1],
-                            (window, 1),
-                        )
-                        for i in range(pairs)
-                    ],
-                    0,
-                )
-                top = jnp.maximum(jnp.max(score, axis=1, keepdims=True), drain)
-                grown = jnp.exp(score - top).astype(BF16)
-                both = dot(grown, two_values)
-                at = 0 if odd else size
-                total = both[:, at : at + 1] + jnp.exp(drain - top)
-                sides.append(both * (1.0 / total))
-            lane = lax.broadcasted_iota(jnp.int32, (tall, 2 * size), 1)
-            both = jnp.where(lane < size, sides[0], sides[1]).astype(BF16)
-            for i in range(pairs):
-                first = (g * share + 2 * i) * size
-                attended[here, first : first + 2 * size] = both[i * window : (i + 1) * window]
-
-    for b in range(token_rows // window):
-        block(at * (token_rows // window) + b)
-
-
-def timeline(count, pieces, favour=None):
-    hop, narrow, tick = 0.6, 0.5, 0.05
-    line_lead, layer_lead = 0.3, 0.6
-    cost = {"pick": 0.07, "expert": 0.67, "mix": 0.08, "pass": 0.02, "norm": 0.02}
+            top = jnp.maximum(jnp.max(score, axis=1, keepdims=True), drain)
+            grown = jnp.exp(score - top).astype(BF16)
+            both = dot(grown, two_values)
+            at = 0 if odd else size
+            total = both[:, at : at + 1] + jnp.exp(drain - top)
+            sides.append(both * (1.0 / total))
+        lane = lax.broadcasted_iota(jnp.int32, (tall, 2 * size), 1)
+        both = jnp.where(lane < size, sides[0], sides[1]).astype(BF16)
+        for i in range(pairs):
+            at = (g * share + 2 * i) * size
+            attended[here, at : at + 2 * size] = both[i * count : (i + 1) * count]
+
+
+def timeline(count, pieces, halves, favour=None):
+    hop, narrow, tick = 0.7, 0.5, 0.05
+    line_lead, layer_lead, begun, spare = 0.3, 0.3, 1.9, 0.3
+    cost = {"close": 0.2, "pick": 0.07, "expert": 0.67, "mix": 0.08, "pass": 0.02}
     every = range(count)
+    bits = [(s, p) for s in every for p in range(halves * pieces)]
     parts = [(s, q) for s in every for q in range(pieces)]
-    landed = {(d, d, q): 0.0 for d in every for q in range(pieces)}
-    came, back, mixed, handed = {}, {}, {}, {}
-    line, layer, busy = {}, [0.0] * count, [0.0] * count
+    landed, came, worked, back, mixed, handed = {}, {}, {}, {}, {}, {}
+    line, layer, busy = {}, [1.1] * count, [begun] * count
     done = [set() for _ in every]
-    steps = [[("norm", d, q) for q in range(pieces)] for d in every]
+    steps = [[] for _ in every]
     now = 0.0
 
-    def put(d, way, at, board, part):
-        line[d, way] = max(line.get((d, way), 0.0), at) + 1
-        board[(d + way,) + part] = line[d, way] + hop
+    def put(d, way, at, board, part, size):
+        line[d, way] = max(line.get((d, way), 0.0), at) + size
+        key = (d + way,) + part
+        board[key] = max(board.get(key, 0.0), line[d, way] + hop)
 
     def there(board, d, part):
         return board.get((d,) + part, now + 1) <= now
+
+    def whole(d, p):
+        return all(there(landed, d, (p[0], h * pieces + p[1])) for h in range(halves))
 
     def choose(d):
         for way, name in ((-1, "send_out"), (1, "send_in")):
             if 0 <= d + way < count and line.get((d, way), 0.0) <= now + line_lead:
                 ready = [
                     p
-                    for p in parts
+                    for p in bits
                     if (p[0] - d) * way <= 0 and there(landed, d, p) and (name, p) not in done[d]
                 ]
                 if ready:
-                    return name, min(ready, key=lambda p: (-abs(p[0] - d), p[1]))
+                    end = d + way in (0, count - 1)
+                    return name, min(ready, key=lambda p: (end and p[0] == d, abs(p[0] - d), p[1]))
+        if ("close", (d, 0)) not in done[d]:
+            return "close", (d, 0)
         ready = [
             p
             for p in parts
@@ -267,11 +268,21 @@
         ]
         if ready:
             return "expert", min(ready, key=lambda p: came[d, p[0], pieces - 1])
-        ready = [p for p in parts if there(landed, d, p) and ("pick", p) not in done[d]]
+        ready = [p for p in parts if whole(d, p) and ("pick", p) not in done[d]]
         if ready and layer[d] <= now + layer_lead:
             return "pick", min(ready, key=lambda p: (favour[d][p[0]] if favour else 0, p))
+        ready = [p for p in parts if p[0] == d and there(worked, d, p) and ("back", p) not in done[d]]
+        if ready and layer[d] <= now:
+            return "back", ready[0]
         return None
 
+    for d in every:
+        for p in range(pieces):
+            landed[d, d, p] = 0.0
+            for way, name in ((-1, "send_out"), (1, "send_in")):
+                if 0 <= d + way < count:
+                    put(d, way, 0.0, landed, (d, p), 1 / halves)
+                    done[d].add((name, (d, p)))
     size = count * pieces
     due = [{"mix": size, "pass": size - pieces if 0 < d < count - 1 else 0} for d in every]
     while any(sum(k == name for k, _ in done[d]) < due[d][name] for d in every for name in due[d]):
@@ -285,24 +296,34 @@
                 steps[d].append((name,) + part)
                 busy[d] = now + cost.get(name, 0.0)
                 if name == "send_in":
-                    put(d, 1, now, landed, part)
+                    put(d, 1, now, landed, part, 1 / halves)
                 elif name == "send_out":
-                    put(d, -1, now, landed, part)
+                    put(d, -1, now, landed, part, 1 / halves)
+                elif name == "close":
+                    for p in range(pieces, halves * pieces):
+                        landed[d, d, p] = busy[d]
                 elif name == "pick":
                     layer[d] = max(layer[d], busy[d]) + narrow
-                    came[(d,) + part] = layer[d] + hop
+                    came[(d,) + part] = layer[d] + hop + (spare if 0 < d < count - 1 else 0)
                 elif name == "expert":
                     for q in range(pieces):
+                        if part[0] == d:
+                            worked[d, d, q] = busy[d]
+                            continue
                         ready = now + cost[name] * (q + 3) / (pieces + 2)
                         layer[d] = max(layer[d], ready) + narrow
                         back[d, part[0], q] = layer[d] + hop
+                elif name == "back":
+                    layer[d] = max(layer[d], now) + narrow
+                    back[(d,) + part] = layer[d] + hop
                 elif name == "mix":
                     mixed[(d,) + part] = busy[d]
                 if name == "pass" or (name == "mix" and part[0] != d and d in (0, count - 1)):
-                    put(d, 1 if part[0] > d else -1, busy[d], handed, part)
+                    put(d, 1 if part[0] > d else -1, busy[d], handed, part, 1)
         now += tick
     if favour is None:
-        return timeline(count, pieces, [[landed[d, s, pieces - 1] for s in every] for d in every])
+        ends = [[landed[d, s, halves * pieces - 1] for s in every] for d in every]
+        return timeline(count, pieces, halves, ends)
     return steps
 
 
@@ -312,21 +333,21 @@
     out,
     queries, residual, seen, attended, halo_send, halo_recv,
     out_w, gate_w, up_w, down_w,
-    pair_out, pair_in, far_out, far_in,
+    pair_out, pair_in, far_out, far_in, mine,
     stream, facts, slots, shares,
     tokens, outbox, arrived, results, returned,
-    local, total_own, line_out, line_in,
-    load_sem, pair_send, pair_recv, far_send, far_recv,
+    local, total_own, line_out, line_in, result,
+    load_sem, out_sem, pair_send, pair_recv, far_send, far_recv,
     facts_send, facts_recv, line_go_send, line_go_recv,
     go_send, go_recv, back_send, back_recv, line_back_send, line_back_recv,
 ):
-    sp_count, tp_count, pieces, capacity = sizes
+    sp_count, tp_count, pieces, halves, capacity = sizes
     chips = tp_count // 2
     z, t = lax.axis_index("sp"), lax.axis_index("tp")
     x, core = t // 2, t % 2
     other = 1 - core
     rows, width = residual_hbm.shape
-    piece = width // pieces
+    piece, half = width // pieces, rows // halves
     top_k = ids.shape[0]
     picks = tp_count * capacity
 
@@ -362,16 +383,6 @@
 
     pad = jnp.zeros((-2 * top_k % 8, rows), F32)
     facts[z] = jnp.concatenate([ids[...].astype(F32), weights[...], pad], 0)
-    pl.semaphore_wait(barrier, sp_count + tp_count - 2)
-    halo_copy = pltpu.make_async_remote_copy(
-        seen.at[pl.ds(reach, WINDOW)], seen.at[pl.ds(0, WINDOW)], halo_send, halo_recv,
-        device_id={"sp": jnp.minimum(z + 1, sp_count - 1)}, device_id_type=MESH,
-    )
-
-    @pl.when(z < sp_count - 1)
-    def _():
-        halo_copy.start()
-
     def facts_copy(k):
         return pltpu.make_async_remote_copy(
             facts.at[z], facts.at[z], facts_send, facts_recv.at[z],
@@ -384,52 +395,79 @@
             device_id={"sp": s}, device_id_type=MESH,
         ).wait_recv()
 
-    for k in range(1, sp_count):
-        facts_copy(k).start()
-
     def route(s):
         slots[s], shares[s] = routing(facts[s], z * tp_count, top_k, tp_count, capacity)
 
-    loads[0].wait()
-
-    def attend_block(at):
-        @pl.when((z > 0) & (at == 0))
+    halo_copy = pltpu.make_async_remote_copy(
+        seen.at[pl.ds(reach, WINDOW)], seen.at[pl.ds(0, WINDOW)], halo_send, halo_recv,
+        device_id={"sp": jnp.minimum(z + 1, sp_count - 1)}, device_id_type=MESH,
+    )
+
+    def attend_half(at, h):
+        attend(z, queries, sink, seen, attended, at * rows + h * half, half)
+
+    def pair_copy(h, k, q):
+        return pltpu.make_async_remote_copy(
+            pair_out.at[h, k, q], pair_in.at[h, k, q], pair_send, pair_recv.at[h, k, q],
+            device_id={"tp": x * 2 + other}, device_id_type=MESH,
+        )
+
+    def far_copy(h, q):
+        return pltpu.make_async_remote_copy(
+            far_out.at[h, q], far_in.at[h, q], far_send, far_recv.at[h, q],
+            device_id={"tp": (1 - x) * 2 + core}, device_id_type=MESH,
+        )
+
+    def give(h, k):
+        block = jnp.concatenate(
+            [
+                attended[pl.ds(pl.multiple_of(at * rows + h * half, half), half), :]
+                for at in ((x + k) % chips * 2 + other, (x + k) % chips * 2 + core)
+            ],
+            0,
+        )
+        for q in range(pieces):
+            both = dot(block, out_w[:, q * piece : (q + 1) * piece])
+            pair_out[h, k, q] = both[:half].astype(BF16)
+            pair_copy(h, k, q).start()
+            mine[h, k, q] = both[half:]
+
+        @pl.when(k > 0)
+        def _():
+            for q in range(pieces):
+                pair_copy(h, k, q).wait_recv()
+                far_out[h, q] = (mine[h, k, q] + pair_in[h, k, q].astype(F32)).astype(BF16)
+                far_copy(h, q).start()
+
+    def turn(h, k):
+        chip = (x + k) % chips
+        attend_half(chip * 2 + 1, h)
+
+        @pl.when((z > 0) & (chip == 0) & (h == 0))
         def _():
             halo_copy.wait_recv()
 
-        attend(z, rows, queries, sink, seen, attended, at)
-
-    def partial(chip, which, q):
-        block = attended[pl.ds(pl.multiple_of((chip * 2 + which) * rows, rows), rows), :]
-        return dot(block, out_w[:, q * piece : (q + 1) * piece])
-
-    def pair_copy(k, q):
-        return pltpu.make_async_remote_copy(
-            pair_out.at[k, q], pair_in.at[k, q], pair_send, pair_recv.at[k, q],
-            device_id={"tp": x * 2 + other}, device_id_type=MESH,
-        )
-
-    def far_copy(k, q):
-        return pltpu.make_async_remote_copy(
-            far_out.at[k, q], far_in.at[k, q], far_send, far_recv.at[k, q],
-            device_id={"tp": ((x + k) % chips) * 2 + core}, device_id_type=MESH,
-        )
-
-    order = list(range(1, chips)) + [0]
-    for k in order:
-        chip = (x + k) % chips
-        attend_block(chip * 2 + other)
-        if k == order[0]:
-            loads[1].wait()
+        attend_half(chip * 2, h)
+        give(h, k)
+
+    def close(h):
+        here = slice(h * half, (h + 1) * half)
+        square = jnp.zeros((half, 1), F32)
         for q in range(pieces):
-            pair_out[k, q] = partial(chip, other, q).astype(BF16)
-            pair_copy(k, q).start()
-        attend_block(chip * 2 + core)
-        for q in range(pieces if k else 0):
-            mine = partial(chip, core, q)
-            pair_copy(k, q).wait_recv()
-            far_out[k, q] = (mine + pair_in[k, q].astype(F32)).astype(BF16)
-            far_copy(k, q).start()
+            cols = slice(q * piece, (q + 1) * piece)
+            total = mine[h, 0, q]
+            pair_copy(h, 0, q).wait_recv()
+            total = total + pair_in[h, 0, q].astype(F32)
+            far_copy(h, q).wait_recv()
+            total = total + far_in[h, q].astype(F32)
+            value = (residual[here, cols].astype(F32) + total).astype(BF16)
+            stream[here, cols] = value
+            value = value.astype(F32)
+            square = square + jnp.sum(value * value, axis=1, keepdims=True)
+        scale = lax.rsqrt(square / width + EPS)
+        for q in range(pieces):
+            cols = slice(q * piece, (q + 1) * piece)
+            tokens[z, q, here, :] = (stream[here, cols].astype(F32) * scale * gain[:, cols]).astype(BF16)
 
     def route_other(k, carry):
         s = (z + k) % sp_count
@@ -437,27 +475,10 @@
         route(s)
         return carry
 
-    route(z)
-    loads[2].wait()
-    lax.fori_loop(1, sp_count, route_other, 0)
-    square = jnp.zeros((rows, 1), F32)
-    for q in range(pieces):
-        cols = slice(q * piece, (q + 1) * piece)
-        total = partial(x, core, q)
-        pair_copy(0, q).wait_recv()
-        total = total + pair_in[0, q].astype(F32)
-        for k in range(1, chips):
-            far_copy(k, q).wait_recv()
-            total = total + far_in[k, q].astype(F32)
-        value = (residual[:, cols].astype(F32) + total).astype(BF16)
-        stream[:, cols] = value
-        value = value.astype(F32)
-        square = square + jnp.sum(value * value, axis=1, keepdims=True)
-    scale = lax.rsqrt(square / width + EPS)
-
-    def line_go(to, s, q):
+    def line_go(to, s, p):
+        bit = tokens.at[s, p % pieces, pl.ds(p // pieces * half, half)]
         return pltpu.make_async_remote_copy(
-            tokens.at[s, q], tokens.at[s, q], line_go_send, line_go_recv.at[s, q],
+            bit, bit, line_go_send, line_go_recv.at[s, p],
             device_id={"sp": to}, device_id_type=MESH,
         )
 
@@ -498,12 +519,42 @@
     def real(s):
         return s + flip * (sp_count - 1 - 2 * s)
 
+    loads[0].wait()
+    attend_half((chips - 1) * 2 + 1, 0)
+    attend_half((chips - 1) * 2, 0)
+    pl.semaphore_wait(barrier, sp_count + tp_count - 2)
+
+    @pl.when(z < sp_count - 1)
+    def _():
+        halo_copy.start()
+
+    for k in range(1, sp_count):
+        facts_copy(k).start()
+    loads[1].wait()
+    give(0, 1 - x)
+
+    def middle(i, carry):
+        turn((1 - x) * (1 - i) + x * i, (1 - i) + x * i)
+        return carry
+
+    lax.fori_loop(0, 2, middle, 0)
+    loads[2].wait()
+    close(0)
+    for p in range(pieces):
+        for way in (-1, 1):
+            @pl.when((place + way >= 0) & (place + way < sp_count))
+            def _():
+                line_go(real(place + way), z, p).start()
+    turn(1, 0)
+    route(z)
+    lax.fori_loop(1, sp_count, route_other, 0)
+
+    def out_copy(q):
+        cols = pl.ds(q * piece, piece)
+        return pltpu.make_async_copy(result.at[:, cols], out.at[:, cols], out_sem.at[q])
+
     def program(m):
         inner, outer = flip, 1 - flip
-
-        def norm(s, q):
-            cols = slice(q * piece, (q + 1) * piece)
-            tokens[z, q] = (stream[:, cols].astype(F32) * scale * gain[:, cols]).astype(BF16)
 
         def land(s, q):
             line_go(real(s), real(s), q).wait_recv()
@@ -535,9 +586,13 @@
             for q in range(pieces):
                 done = dot(hidden, down_w[:, q * piece : (q + 1) * piece]).astype(BF16)
                 results[r, q] = done.reshape(tp_count, capacity, piece)
-                for to in peers:
-                    back_copy(r, q, to, t).start()
+                if s != m:
+                    give_back(s, q)
                 returned[r, q, t] = results[r, q, t]
+
+        def give_back(s, q):
+            for to in peers:
+                back_copy(real(s), q, to, t).start()
 
         def mix(s, q):
             r = real(s)
@@ -560,8 +615,8 @@
             line_back(real(to), r, q, way).start()
 
         act = {
-            "norm": norm, "send_in": send_in, "send_out": send_out,
-            "pick": pick, "expert": expert, "mix": mix, "pass": hand_on,
+            "close": lambda *_: close(1), "send_in": send_in, "send_out": send_out,
+            "pick": pick, "expert": expert, "back": give_back, "mix": mix, "pass": hand_on,
         }
         waited = set()
         for name, s, q in steps[m]:
@@ -569,22 +624,24 @@
                 waited.add("loads")
                 for load in loads[3:]:
                     load.wait()
-            if name in ("pick", "send_in", "send_out") and s != m and (s, q) not in waited:
-                waited.add((s, q))
-                land(s, q)
+            for p in range(q, halves * pieces, pieces) if name == "pick" else [q]:
+                if name in ("pick", "send_in", "send_out") and s != m and (s, p) not in waited:
+                    waited.add((s, p))
+                    land(s, p)
             act[name](s, q)
         for q in range(pieces):
             total = total_own[q]
             for way in [inner, outer] if m > 0 else [outer]:
                 line_back(real(m + 1), z, q, way).wait_recv()
                 total = total + line_in[way, z, q].astype(F32)
-            out[:, q * piece : (q + 1) * piece] = total.astype(BF16)
+            result[:, q * piece : (q + 1) * piece] = total.astype(BF16)
+            out_copy(q).start()
         peer = {"sp": real(m + 1)}
         for _ in range(sp_count + 1 if m > 0 else 1):
             sent(tokens.at[0], line_go_send, peer)
         sent(line_out.at[pl.ds(0, sp_count - 1)], line_back_send, peer)
 
-    steps = timeline(sp_count, pieces)
+    steps = timeline(sp_count, pieces, halves)
     for m in range((sp_count + 1) // 2):
         pl.when(place == m)(functools.partial(program, m))
 
@@ -595,9 +652,11 @@
     peer = {"tp": x * 2 + other}
     sent(facts.at[pl.ds(0, sp_count - 1)], facts_send, {"sp": (z + 1) % sp_count})
     sent(pair_out, pair_send, peer)
-    sent(far_out.at[pl.ds(1, chips - 1)], far_send, peer)
+    sent(far_out, far_send, peer)
     sent(outbox.at[:, :, pl.ds(0, tp_count - 1)], go_send, peer)
     sent(results.at[:, :, pl.ds(0, tp_count - 1)], back_send, peer)
+    for q in range(pieces):
+        out_copy(q).wait()
 
 
 def fused(
@@ -611,10 +670,10 @@
     capacity = max(2, 2 * top_k * rows // experts)
     hidden = gate_weight.shape[2]
     depth = out_weight.shape[0]
-    pieces = 4
+    pieces, halves = 4, 2
     chips = tp_count // 2
     piece = width // pieces
-    part = (chips, pieces, rows, piece)
+    part = (halves, chips, pieces, rows // halves, piece)
     line = (sp_count, pieces, rows, piece)
     box = (sp_count, pieces, tp_count, capacity, piece)
     picks = tp_count * capacity
@@ -624,10 +683,10 @@
     hbm = pl.BlockSpec(memory_space=pl.ANY)
     dma = pltpu.SemaphoreType.DMA
     return pl.pallas_call(
-        functools.partial(tail_kernel, (sp_count, tp_count, pieces, capacity)),
+        functools.partial(tail_kernel, (sp_count, tp_count, pieces, halves, capacity)),
         out_shape=jax.ShapeDtypeStruct((rows, width), BF16),
         in_specs=[hbm, vmem, vmem, vmem, hbm, hbm, vmem, vmem, vmem, hbm, hbm, hbm],
-        out_specs=vmem,
+        out_specs=hbm,
         scratch_shapes=[
             pltpu.VMEM(queries.shape, BF16),
             pltpu.VMEM(residual.shape, BF16),
@@ -641,8 +700,9 @@
             pltpu.VMEM((hidden, width), BF16),
             pltpu.VMEM(part, BF16),
             pltpu.VMEM(part, BF16),
-            pltpu.VMEM(part, BF16),
-            pltpu.VMEM(part, BF16),
+            pltpu.VMEM(part[:1] + part[2:], BF16),
+            pltpu.VMEM(part[:1] + part[2:], BF16),
+            pltpu.VMEM(part, F32),
             pltpu.VMEM((rows, width), BF16),
             pltpu.VMEM((sp_count, 2 * top_k + -2 * top_k % 8, rows), F32),
             pltpu.VMEM((sp_count, picks, rows), BF16),
@@ -656,15 +716,17 @@
             pltpu.VMEM(line[1:], F32),
             pltpu.VMEM(line, BF16),
             pltpu.VMEM((2,) + line, BF16),
+            pltpu.VMEM((rows, width), BF16),
             dma((6,)),
-            dma,
-            dma((chips, pieces)),
-            dma,
-            dma((chips, pieces)),
+            dma((pieces,)),
+            dma,
+            dma((halves, chips, pieces)),
+            dma,
+            dma((halves, pieces)),
             dma,
             dma((sp_count,)),
             dma,
-            dma((sp_count, pieces)),
+            dma((sp_count, halves * pieces)),
             dma,
             dma((sp_count, pieces)),
             dma,
@@ -685,7 +747,7 @@
     rows_dev = rest[1].shape[0]
     experts = lax.axis_size("sp") * lax.axis_size("tp")
     fits = 2 * rest[3].shape[1] * rows_dev // experts % 16 == 0 and rows_dev % WINDOW == 0
-    fits = fits and lax.axis_size("sp") > 1 and lax.axis_size("tp") > 2
+    fits = fits and lax.axis_size("sp") > 1 and lax.axis_size("tp") == 4
     if fits:
         return fused(queries, key_heads, value_heads, sink_logit, *rest)
     return tail_plain(attention(queries, key_heads, value_heads, sink_logit), *rest)

time: 95.6 us -> 89.1 us (0.932)
  Pallas kernels: 93.5 us -> 87 us
    pallas_call x1, Pallas kernels: 93.5 us -> 87 us  [fused(): pl.pallas_call(functools.partial(tail_kernel, (sp_count, tp_count, pieces...]
where the time goes in v3:
time: 89.1 us; the launch traced here: 88.9 us
  Pallas kernels  87 us (98%)
  local copies, waits for them, and re-layouts  1.88 us (2%)
    pallas_call x1, Pallas kernels, fused(): pl.pallas_call(functools.partial(tail_kernel, (sp_count, tp_count, pieces...  87 us
    unnamed x1, local copies, waits for them, and re-layouts  1.88 us

profile of v3, /device:TPU:0, one launch (start us, length us, event | category | flops | bytes accessed | tf_op | source)
XLA Modules:
  0.0 88.9 jit_solution(17037696652590755947)
XLA Ops:
  0.0 87.0 %shard_map.118 = bf16[128,2048]{1,0:T(8,128)(2,1)} custom-call(bf16[512,512]{1,0:T(8,128)(2,1)} %queries_hbm.1, bf16[1,64,512]{2,1,0:T(8,128)(2,1)} %bitcast.6, bf16[1,64,512]{2,1,0:T(8,128)(2,1)} %bitcast.7, f32[1,8]{1,0:T(1,128)} %bitcast.11, bf16[512,2048]{1,0:T(8,128)(2,1)} %out_w_hbm.1, bf16[128,2048]{1,0:T(8,128)(2,1)} %residual_hbm.1, ...), custom_call_target="tpu_custom_call" | custom-call | tf_op jit(solution)/shard_map/pallas_call | solution.py:685
  87.0 1.9 %copy.14 = bf16[128,2048]{1,0:T(8,128)(2,1)} copy(bf16[128,2048]{1,0:T(8,128)(2,1)} %shard_map.118) | data formatting | bytes 1048576

commit v4 on v3

--- a/solution.py
+++ b/solution.py
@@ -15,7 +15,7 @@
 F32 = jnp.float32
 BF16 = jnp.bfloat16
 MESH = pl.DeviceIdType.MESH
-VMEM_BUDGET = 56 * 1024 * 1024
+VMEM_BUDGET = 54 * 1024 * 1024
 
 
 def from_behind(value, axis, steps):
@@ -329,15 +329,16 @@
 
 def tail_kernel(
     sizes,
-    queries_hbm, keys, values, sink, out_w_hbm, residual_hbm, gain, ids, weights, gate_hbm, up_hbm, down_hbm,
+    queries_hbm, keys_hbm, values_hbm, sink_hbm, out_w_hbm, residual_hbm, gain_hbm, ids_hbm, weights_hbm,
+    gate_hbm, up_hbm, down_hbm,
     out,
-    queries, residual, seen, attended, halo_send, halo_recv,
+    queries, keys, values, sink, residual, gain, ids, weights, seen, attended, halo_send, halo_recv,
     out_w, gate_w, up_w, down_w,
     pair_out, pair_in, far_out, far_in, mine,
     stream, facts, slots, shares,
     tokens, outbox, arrived, results, returned,
-    local, total_own, line_out, line_in, result,
-    load_sem, out_sem, pair_send, pair_recv, far_send, far_recv,
+    local, total_own, line_out, line_in,
+    load_sem, pair_send, pair_recv, far_send, far_recv,
     facts_send, facts_recv, line_go_send, line_go_recv,
     go_send, go_recv, back_send, back_recv, line_back_send, line_back_recv,
 ):
@@ -348,7 +349,7 @@
     other = 1 - core
     rows, width = residual_hbm.shape
     piece, half = width // pieces, rows // halves
-    top_k = ids.shape[0]
+    top_k = ids_hbm.shape[0]
     picks = tp_count * capacity
 
     barrier = pltpu.get_barrier_semaphore()
@@ -364,8 +365,9 @@
         pltpu.make_async_copy(src, dst, load_sem.at[i])
         for i, (src, dst) in enumerate(
             (
-                (queries_hbm, queries), (out_w_hbm, out_w), (residual_hbm, residual),
-                (gate_hbm.at[0], gate_w), (up_hbm.at[0], up_w), (down_hbm.at[0], down_w),
+                (keys_hbm, keys), (values_hbm, values), (queries_hbm, queries), (sink_hbm, sink),
+                (ids_hbm, ids), (weights_hbm, weights), (out_w_hbm, out_w), (residual_hbm, residual),
+                (gain_hbm, gain), (gate_hbm.at[0], gate_w), (up_hbm.at[0], up_w), (down_hbm.at[0], down_w),
             )
         )
     ]
@@ -373,6 +375,8 @@
         load.start()
 
     groups, size, reach = keys.shape
+    for load in loads[:2]:
+        load.wait()
     for g in range(groups):
         both = jnp.concatenate([keys[g], values[g]], 0)
         seen[WINDOW:, 2 * g * size : (2 * g + 2) * size] = both.T
@@ -381,6 +385,8 @@
     def _():
         seen[:WINDOW, :] = jnp.zeros((WINDOW, seen.shape[1]), BF16)
 
+    for load in loads[2:6]:
+        load.wait()
     pad = jnp.zeros((-2 * top_k % 8, rows), F32)
     facts[z] = jnp.concatenate([ids[...].astype(F32), weights[...], pad], 0)
     def facts_copy(k):
@@ -418,35 +424,54 @@
             device_id={"tp": (1 - x) * 2 + core}, device_id_type=MESH,
         )
 
+    def far_out_all(h):
+        for q in range(pieces):
+            pair_copy(h, 1, q).wait_recv()
+            far_out[h, q] = (mine[h, 1, q] + pair_in[h, 1, q].astype(F32)).astype(BF16)
+            far_copy(h, q).start()
+
+    def taken(at, h):
+        return attended[pl.ds(pl.multiple_of(at * rows + h * half, half), half), :]
+
     def give(h, k):
-        block = jnp.concatenate(
-            [
-                attended[pl.ds(pl.multiple_of(at * rows + h * half, half), half), :]
-                for at in ((x + k) % chips * 2 + other, (x + k) % chips * 2 + core)
-            ],
-            0,
-        )
+        chip = (x + k) % chips
+        block = jnp.concatenate([taken(chip * 2 + other, h), taken(chip * 2 + core, h)], 0)
         for q in range(pieces):
             both = dot(block, out_w[:, q * piece : (q + 1) * piece])
             pair_out[h, k, q] = both[:half].astype(BF16)
             pair_copy(h, k, q).start()
             mine[h, k, q] = both[half:]
-
-        @pl.when(k > 0)
+        if k:
+            far_out_all(h)
+
+    def give_one(h, at):
+        block = taken(at, h)
+        for q in range(pieces):
+            one = dot(block, out_w[:, q * piece : (q + 1) * piece])
+
+            @pl.when(at % 2 == core)
+            def _():
+                mine[h, 1, q] = one
+
+            @pl.when(at % 2 == other)
+            def _():
+                pair_out[h, 1, q] = one.astype(BF16)
+                pair_copy(h, 1, q).start()
+
+        @pl.when(at % 2 == core)
         def _():
-            for q in range(pieces):
-                pair_copy(h, k, q).wait_recv()
-                far_out[h, q] = (mine[h, k, q] + pair_in[h, k, q].astype(F32)).astype(BF16)
-                far_copy(h, q).start()
+            far_out_all(h)
+
+    def first_rows():
+        @pl.when(z > 0)
+        def _():
+            halo_copy.wait_recv()
+
+        attend_half(0, 0)
 
     def turn(h, k):
         chip = (x + k) % chips
         attend_half(chip * 2 + 1, h)
-
-        @pl.when((z > 0) & (chip == 0) & (h == 0))
-        def _():
-            halo_copy.wait_recv()
-
         attend_half(chip * 2, h)
         give(h, k)
 
@@ -482,10 +507,10 @@
             device_id={"sp": to}, device_id_type=MESH,
         )
 
-    def line_back(to, s, q, way):
+    def line_back(to, s, q, way, last=False):
         return pltpu.make_async_remote_copy(
             line_out.at[s, q], line_in.at[way, s, q], line_back_send,
-            line_back_recv.at[way, s, q], device_id={"sp": to}, device_id_type=MESH,
+            line_back_recv.at[s + last * way * (sp_count - s), q], device_id={"sp": to}, device_id_type=MESH,
         )
 
     def go_copy(s, q, to, at):
@@ -519,7 +544,6 @@
     def real(s):
         return s + flip * (sp_count - 1 - 2 * s)
 
-    loads[0].wait()
     attend_half((chips - 1) * 2 + 1, 0)
     attend_half((chips - 1) * 2, 0)
     pl.semaphore_wait(barrier, sp_count + tp_count - 2)
@@ -530,15 +554,29 @@
 
     for k in range(1, sp_count):
         facts_copy(k).start()
-    loads[1].wait()
-    give(0, 1 - x)
-
-    def middle(i, carry):
-        turn((1 - x) * (1 - i) + x * i, (1 - i) + x * i)
-        return carry
-
-    lax.fori_loop(0, 2, middle, 0)
-    loads[2].wait()
+    loads[6].wait()
+
+    @pl.when(x == 0)
+    def _():
+        give(0, 1)
+
+    @pl.when(x == 1)
+    def _():
+        attend_half(1, 0)
+        give_one(0, 1)
+        first_rows()
+        give_one(0, 0)
+
+    turn(1, 1)
+
+    @pl.when(x == 0)
+    def _():
+        attend_half(1, 0)
+        first_rows()
+
+    give(0, 0)
+    for load in loads[7:9]:
+        load.wait()
     close(0)
     for p in range(pieces):
         for way in (-1, 1):
@@ -548,10 +586,6 @@
     turn(1, 0)
     route(z)
     lax.fori_loop(1, sp_count, route_other, 0)
-
-    def out_copy(q):
-        cols = pl.ds(q * piece, piece)
-        return pltpu.make_async_copy(result.at[:, cols], out.at[:, cols], out_sem.at[q])
 
     def program(m):
         inner, outer = flip, 1 - flip
@@ -603,7 +637,7 @@
                 total_own[q] = stream[:, q * piece : (q + 1) * piece].astype(F32) + mixed
             elif m == 0:
                 line_out[r, q] = mixed.astype(BF16)
-                line_back(real(1), r, q, inner).start()
+                line_back(real(1), r, q, inner, s == 1).start()
             else:
                 local[r, q] = mixed
 
@@ -612,7 +646,7 @@
             way, to = (inner, m + 1) if s > m else (outer, m - 1)
             line_back(real(to), r, q, way).wait_recv()
             line_out[r, q] = (local[r, q] + line_in[way, r, q].astype(F32)).astype(BF16)
-            line_back(real(to), r, q, way).start()
+            line_back(real(to), r, q, way, s == to).start()
 
         act = {
             "close": lambda *_: close(1), "send_in": send_in, "send_out": send_out,
@@ -622,7 +656,7 @@
         for name, s, q in steps[m]:
             if name == "expert" and "loads" not in waited:
                 waited.add("loads")
-                for load in loads[3:]:
+                for load in loads[9:]:
                     load.wait()
             for p in range(q, halves * pieces, pieces) if name == "pick" else [q]:
                 if name in ("pick", "send_in", "send_out") and s != m and (s, p) not in waited:
@@ -632,10 +666,9 @@
         for q in range(pieces):
             total = total_own[q]
             for way in [inner, outer] if m > 0 else [outer]:
-                line_back(real(m + 1), z, q, way).wait_recv()
+                line_back(real(m + 1), z, q, way, True).wait_recv()
                 total = total + line_in[way, z, q].astype(F32)
-            result[:, q * piece : (q + 1) * piece] = total.astype(BF16)
-            out_copy(q).start()
+            out[:, q * piece : (q + 1) * piece] = total.astype(BF16)
         peer = {"sp": real(m + 1)}
         for _ in range(sp_count + 1 if m > 0 else 1):
             sent(tokens.at[0], line_go_send, peer)
@@ -655,8 +688,6 @@
     sent(far_out, far_send, peer)
     sent(outbox.at[:, :, pl.ds(0, tp_count - 1)], go_send, peer)
     sent(results.at[:, :, pl.ds(0, tp_count - 1)], back_send, peer)
-    for q in range(pieces):
-        out_copy(q).wait()
 
 
 def fused(
@@ -680,16 +711,22 @@
     reach, groups, size = key_heads.shape
     keys, values = key_heads.transpose(1, 2, 0), value_heads.transpose(1, 2, 0)
     vmem = pl.BlockSpec(memory_space=pltpu.VMEM)
-    hbm = pl.BlockSpec(memory_space=pl.ANY)
+    hbm = pl.BlockSpec(memory_space=pltpu.MemorySpace.HBM)
     dma = pltpu.SemaphoreType.DMA
     return pl.pallas_call(
         functools.partial(tail_kernel, (sp_count, tp_count, pieces, halves, capacity)),
-        out_shape=jax.ShapeDtypeStruct((rows, width), BF16),
-        in_specs=[hbm, vmem, vmem, vmem, hbm, hbm, vmem, vmem, vmem, hbm, hbm, hbm],
-        out_specs=hbm,
+        out_shape=pltpu.VMEM((rows, width), BF16),
+        in_specs=[hbm] * 12,
+        out_specs=vmem,
         scratch_shapes=[
             pltpu.VMEM(queries.shape, BF16),
+            pltpu.VMEM(keys.shape, BF16),
+            pltpu.VMEM(values.shape, BF16),
+            pltpu.VMEM((1,) + sink_logit.shape, F32),
             pltpu.VMEM(residual.shape, BF16),
+            pltpu.VMEM((1,) + norm_gain.shape, F32),
+            pltpu.VMEM((top_k, rows), jnp.int32),
+            pltpu.VMEM((top_k, rows), F32),
             pltpu.VMEM((WINDOW + reach, groups * 2 * size), BF16),
             pltpu.VMEM(queries.shape, BF16),
             dma,
@@ -716,9 +753,7 @@
             pltpu.VMEM(line[1:], F32),
             pltpu.VMEM(line, BF16),
             pltpu.VMEM((2,) + line, BF16),
-            pltpu.VMEM((rows, width), BF16),
-            dma((6,)),
-            dma((pieces,)),
+            dma((12,)),
             dma,
             dma((halves, chips, pieces)),
             dma,
@@ -732,7 +767,7 @@
             dma,
             dma((sp_count, pieces)),
             dma,
-            dma((2, sp_count, pieces)),
+            dma((sp_count + 1, pieces)),
         ],
         compiler_params=pltpu.CompilerParams(
             collective_id=0, has_side_effects=True, vmem_limit_bytes=VMEM_BUDGET

time: 89.1 us -> 84.9 us (0.953)
  Pallas kernels: 87 us -> 83.9 us
  local copies, waits for them, and re-layouts: 1.88 us -> 0.8 us
    pallas_call x1, Pallas kernels: 87 us -> 83.9 us  [fused(): pl.pallas_call(functools.partial(tail_kernel, (sp_count, tp_count, pieces...]
    unnamed x1, local copies, waits for them, and re-layouts: 1.88 us -> 0.8 us
where the time goes in v4:
time: 84.9 us; the launch traced here: 84.7 us
  Pallas kernels  83.9 us (99%)
    pallas_call x1, Pallas kernels, fused(): pl.pallas_call(functools.partial(tail_kernel, (sp_count, tp_count, pieces...  83.9 us

profile of v4, /device:TPU:0, one launch (start us, length us, event | category | flops | bytes accessed | tf_op | source)
XLA Modules:
  0.0 84.7 jit_solution(3949684885590822778)
XLA Ops:
  0.0 83.9 %shard_map.118 = bf16[128,2048]{1,0:T(8,128)(2,1)S(1)} custom-call(bf16[512,512]{1,0:T(8,128)(2,1)} %queries_hbm.1, bf16[1,64,512]{2,1,0:T(8,128)(2,1)} %bitcast.6, bf16[1,64,512]{2,1,0:T(8,128)(2,1)} %bitcast.7, f32[1,8]{1,0:T(1,128)} %bitcast.11, bf16[512,2048]{1,0:T(8,128)(2,1)} %out_w_hbm.1, bf16[128,2048]{1,0:T(8,128)(2,1)} %residual_hbm.1, ...), custom_call_target="tpu_custom_call" | custom-call | tf_op jit(solution)/shard_map/pallas_call | solution.py:716
  83.9 0.8 copy.14

commit v5 on v4

--- a/solution.py
+++ b/solution.py
@@ -216,7 +216,7 @@
 
 def timeline(count, pieces, halves, favour=None):
     hop, narrow, tick = 0.7, 0.5, 0.05
-    line_lead, layer_lead, begun, spare = 0.3, 0.3, 1.9, 0.3
+    line_lead, layer_lead, begun, spare = 0.3, 0.6, 1.9, 0.3
     cost = {"close": 0.2, "pick": 0.07, "expert": 0.67, "mix": 0.08, "pass": 0.02}
     every = range(count)
     bits = [(s, p) for s in every for p in range(halves * pieces)]
@@ -272,7 +272,8 @@
         if ready and layer[d] <= now + layer_lead:
             return "pick", min(ready, key=lambda p: (favour[d][p[0]] if favour else 0, p))
         ready = [p for p in parts if p[0] == d and there(worked, d, p) and ("back", p) not in done[d]]
-        if ready and layer[d] <= now:
+        ahead = [s for s in every if s != d and ("expert", (s, 0)) not in done[d]]
+        if ready and layer[d] <= now and not ahead:
             return "back", ready[0]
         return None
 

time: 84.9 us -> 83.7 us (0.986)
  Pallas kernels: 83.9 us -> 82.7 us
    pallas_call x1, Pallas kernels: 83.9 us -> 82.7 us  [fused(): pl.pallas_call(functools.partial(tail_kernel, (sp_count, tp_count, pieces...]
where the time goes in v5:
time: 83.7 us; the launch traced here: 83.5 us
  Pallas kernels  82.7 us (99%)
    pallas_call x1, Pallas kernels, fused(): pl.pallas_call(functools.partial(tail_kernel, (sp_count, tp_count, pieces...  82.7 us

profile of v5, /device:TPU:0, one launch (start us, length us, event | category | flops | bytes accessed | tf_op | source)
XLA Modules:
  0.0 83.5 jit_solution(660652920003011250)
XLA Ops:
  0.0 82.7 %shard_map.118 = bf16[128,2048]{1,0:T(8,128)(2,1)S(1)} custom-call(bf16[512,512]{1,0:T(8,128)(2,1)} %queries_hbm.1, bf16[1,64,512]{2,1,0:T(8,128)(2,1)} %bitcast.6, bf16[1,64,512]{2,1,0:T(8,128)(2,1)} %bitcast.7, f32[1,8]{1,0:T(1,128)} %bitcast.11, bf16[512,2048]{1,0:T(8,128)(2,1)} %out_w_hbm.1, bf16[128,2048]{1,0:T(8,128)(2,1)} %residual_hbm.1, ...), custom_call_target="tpu_custom_call" | custom-call | tf_op jit(solution)/shard_map/pallas_call | solution.py:717
  82.7 0.8 copy.14
